TPU v7x, 256 devices: a whole 4x4x8 slice. The times are simulated.
256 devices in a mesh: ep: 16 (over y, x), tp: 16 (over z, core).
Axes of the slice: x: 4, y: 4, z: 8, core: 2. Of those that a mesh axis runs over, the one named last changes fastest.
Arguments:
- tokens: bfloat16 [1024, 4096], P(('ep', 'tp')), may hold values from -6 to 6
- rec_state: float32 [1024, 2048], P('ep', 'tp'), may hold values from -40 to 40
- conv_state: bfloat16 [1024, 3, 2048], P('ep', None, 'tp'), may hold values from -6 to 6
- route_ids: int32 [1024, 4], P('ep'), may hold values from 0 to 15, all different within a row; in each aligned block of 4 rows (0 to 3, 4 to 7, ...) at most 2 rows name the same one
- route_weights: float32 [1024, 4], P(('ep', 'tp')), may hold values from 0.1 to 1
- first_gain: bfloat16 [4096], replicated, may hold values from 0.099609375 to 1.8984375
- proj_input: bfloat16 [4096, 2048], P(None, 'tp'), may hold values from -0.09375 to 0.09375
- proj_gate: bfloat16 [4096, 2048], P(None, 'tp'), may hold values from -0.09375 to 0.09375
- conv_taps: bfloat16 [4, 2048], replicated, may hold values from -1.5 to 1.5
- decay_logit: float32 [2048], replicated, may hold values from 1 to 6
- block_decay: bfloat16 [16, 128, 128], replicated, may hold values from -0.5 to 0.5
- block_input: bfloat16 [16, 128, 128], replicated, may hold values from -0.5 to 0.5
- rec_gain: bfloat16 [2048], replicated, may hold values from 0.099609375 to 1.8984375
- proj_out: bfloat16 [2048, 4096], P('tp'), may hold values from -0.125 to 0.125
- second_gain: bfloat16 [4096], replicated, may hold values from 0.099609375 to 1.8984375
- expert_gate: bfloat16 [16, 4096, 4096], P('ep', None, 'tp'), may hold values from -0.21875 to 0.21875
- expert_up: bfloat16 [16, 4096, 4096], P('ep', None, 'tp'), may hold values from -0.21875 to 0.21875
- expert_down: bfloat16 [16, 4096, 4096], P('ep', 'tp'), may hold values from -0.0234375 to 0.0234375
Outputs:
- result: bfloat16 [1024, 4096], P(('ep', 'tp'))
- new_state: float32 [1024, 2048], P('ep', 'tp')
- new_conv: bfloat16 [1024, 3, 2048], P('ep', None, 'tp')
Inputs may be any that keep to these rules, and one draw needn't show every extreme that they name: `route_ids`: each row names 4 different experts; in the rows of one device (aligned blocks of 4 rows) no expert is named by more than 2 rows, and one is named by exactly 2.
All inputs are finite; a program needn't handle non-finite values.
Results may differ from a plain program's by a relative error of at most 0.025.
Values may be sent and summed in bfloat16 or wider, within the bound.
A program may use at most 64 MiB of HBM per device.

v0:
```python
import jax
import jax.numpy as jnp
from jax import lax
from jax.sharding import PartitionSpec as P

EXPERTS = 16


EPS = 1e-06
CLAMP = 7.0
ALPHA = 1.702
RATE = 8.0


def in_order(tiles, dim):
    lengths = list(tiles.shape[1:])
    lengths[dim] *= tiles.shape[0]
    return jnp.moveaxis(tiles, 0, dim).reshape(lengths)


def sent_to_all(shard, axis):
    size = lax.axis_size(axis)
    return lax.all_to_all(
        jnp.broadcast_to(shard[None], (size, *shard.shape)), axis, 0, 0, tiled=True
    )


def gather_directly(shard, axis, dim):
    return in_order(sent_to_all(shard, axis), dim)


def split_up(shard, dim, size):
    before, after = (shard.shape[:dim], shard.shape[dim + 1 :])
    return jnp.moveaxis(shard.reshape(*before, size, -1, *after), dim, 0)


def summed_on_arrival(shard, axis, dim):
    size = lax.axis_size(axis)
    tiles = lax.all_to_all(split_up(shard, dim, size), axis, 0, 0, tiled=True)
    return jnp.sum(tiles.astype(jnp.float32), axis=0)


def side_by_side(arrays, axis, dim, along):
    both = jnp.concatenate(arrays, axis=along)
    out, at, outs = (summed_on_arrival(both, axis, dim), 0, [])
    for a in arrays:
        outs.append(lax.slice_in_dim(out, at, at + a.shape[along], axis=along))
        at += a.shape[along]
    return tuple(outs)


def norm_rows(values, gain):
    scale = lax.rsqrt(jnp.mean(values * values, axis=-1, keepdims=True) + EPS)
    return values * scale * gain.astype(jnp.float32)


def slot_positions(ids, blocks):
    rows, picks = ids.shape
    onehot = (ids[:, :, None] == jnp.arange(EXPERTS, dtype=jnp.int32)).astype(jnp.int32)
    onehot = onehot.reshape(blocks, rows // blocks * picks, EXPERTS)
    before = jnp.cumsum(onehot, axis=1) - onehot
    return jnp.sum(before * onehot, axis=-1).reshape(rows, picks)


def dispatch_rows(slots, rows_in, total):
    hits = (slots[:, :, None] == jnp.arange(total, dtype=jnp.int32)).astype(jnp.bfloat16)
    chooser = jnp.sum(hits, axis=1)
    return jnp.einsum("ns,nd->sd", chooser, rows_in, preferred_element_type=jnp.float32).astype(
        jnp.bfloat16
    )


def run_experts(piece, expert_gate, expert_up, expert_down):
    gate = jnp.einsum("erd,edf->erf", piece, expert_gate, preferred_element_type=jnp.float32)
    upper = jnp.einsum("erd,edf->erf", piece, expert_up, preferred_element_type=jnp.float32)
    clipped = jnp.minimum(gate, CLAMP)
    act = (
        (jnp.clip(upper, -CLAMP, CLAMP) + 1.0) * (clipped * jax.nn.sigmoid(ALPHA * clipped))
    ).astype(jnp.bfloat16)
    return jnp.einsum("erf,efd->erd", act, expert_down, preferred_element_type=jnp.float32)


def per_device(
    tokens,
    rec_state,
    conv_state,
    route_ids,
    route_weights,
    first_gain,
    proj_input,
    proj_gate,
    conv_taps,
    decay_logit,
    block_decay,
    block_input,
    rec_gain,
    proj_out,
    second_gain,
    expert_gate,
    expert_up,
    expert_down,
):
    tp_count = lax.axis_size("tp")
    tp_place = lax.axis_index("tp")
    local_width = proj_input.shape[1]
    seq_count = rec_state.shape[0]
    own_count = tokens.shape[0]
    top_count = route_ids.shape[1]
    capacity = max(2, own_count * top_count // EXPERTS)
    first_channel = tp_place * local_width
    own_values = tokens.astype(jnp.float32)
    normed = norm_rows(own_values, first_gain).astype(jnp.bfloat16)
    piece = gather_directly(normed, "tp", 0)
    both = jnp.concatenate(
        [
            jnp.dot(piece, proj_input, preferred_element_type=jnp.float32),
            jnp.dot(piece, proj_gate, preferred_element_type=jnp.float32),
        ],
        axis=1,
    )
    joined = both.astype(jnp.bfloat16)
    branch_in = joined[:, :local_width]
    branch_gate = joined[:, local_width:]
    tap_weights = lax.dynamic_slice_in_dim(conv_taps, first_channel, local_width, 1).astype(
        jnp.float32
    )
    conv_values = conv_state.astype(jnp.float32)
    conv_output = tap_weights[-1] * branch_in.astype(jnp.float32)
    for tap in range(conv_state.shape[1]):
        conv_output = conv_output + tap_weights[tap] * conv_values[:, tap]
    new_conv = jnp.concatenate([conv_state[:, 1:], branch_in[:, None, :]], axis=1)
    block_width = block_decay.shape[1]
    local_blocks = local_width // block_width
    decay_mats = lax.dynamic_slice_in_dim(block_decay, tp_place * local_blocks, local_blocks, 0)
    input_mats = lax.dynamic_slice_in_dim(block_input, tp_place * local_blocks, local_blocks, 0)
    blocked = conv_output.astype(jnp.bfloat16).reshape(seq_count, local_blocks, block_width)
    decay_gate = jax.nn.sigmoid(
        jnp.einsum("rnk,nkj->rnj", blocked, decay_mats, preferred_element_type=jnp.float32).reshape(
            seq_count, local_width
        )
    )
    input_gate = jax.nn.sigmoid(
        jnp.einsum("rnk,nkj->rnj", blocked, input_mats, preferred_element_type=jnp.float32).reshape(
            seq_count, local_width
        )
    )
    decay_logits = lax.dynamic_slice_in_dim(decay_logit, first_channel, local_width, 0)
    log_keep = -RATE * decay_gate * jax.nn.softplus(-decay_logits)
    keep_factor = jnp.exp(log_keep)
    fresh_input = jnp.sqrt(-jnp.expm1(2.0 * log_keep)) * input_gate * conv_output
    new_state = keep_factor * rec_state + fresh_input
    hidden = new_state * jax.nn.gelu(branch_gate.astype(jnp.float32))
    squares = jnp.sum(hidden * hidden, axis=1, keepdims=True)
    gain_part = lax.dynamic_slice_in_dim(rec_gain, first_channel, local_width, 0).astype(
        jnp.float32
    )
    partial_value = jnp.dot(
        (hidden * gain_part).astype(jnp.bfloat16), proj_out, preferred_element_type=jnp.float32
    )
    channels = local_width * tp_count
    width_out = proj_out.shape[1]
    own_ids = lax.dynamic_slice_in_dim(route_ids, tp_place * own_count, own_count, 0)
    own_slots = own_ids * capacity + slot_positions(own_ids, 1)
    mix_part, own_squares = side_by_side(
        (partial_value.astype(jnp.bfloat16), squares.astype(jnp.bfloat16)), "tp", 0, 1
    )
    residual = own_values + mix_part * lax.rsqrt(own_squares / channels + EPS)
    second_normed = norm_rows(residual, second_gain).astype(jnp.bfloat16)
    outgoing = dispatch_rows(own_slots, second_normed, EXPERTS * capacity).reshape(
        EXPERTS, capacity, width_out
    )
    arrived = lax.all_to_all(outgoing, "ep", split_axis=0, concat_axis=1, tiled=True)
    partials = run_experts(
        lax.all_gather(arrived, "tp", axis=1, tiled=True), expert_gate, expert_up, expert_down
    )
    summed_rows = lax.psum_scatter(
        partials.astype(jnp.bfloat16), "tp", scatter_dimension=1, tiled=True
    )
    returned = lax.all_to_all(summed_rows, "ep", split_axis=1, concat_axis=0, tiled=True)
    returned_rows = returned.reshape(EXPERTS * capacity, width_out).astype(jnp.float32)
    slot_hits = (own_slots[:, :, None] == jnp.arange(EXPERTS * capacity, dtype=jnp.int32)).astype(
        jnp.float32
    )
    combine_weights = jnp.sum(slot_hits * route_weights[:, :, None], axis=1)
    expert_mix = jnp.dot(combine_weights, returned_rows, precision=lax.Precision.HIGHEST)
    result = (residual + expert_mix).astype(jnp.bfloat16)
    return (result, new_state, new_conv)


def solution(mesh):
    in_specs = (
        P(("ep", "tp"), None),
        P("ep", "tp"),
        P("ep", None, "tp"),
        P("ep", None),
        P(("ep", "tp"), None),
        P(),
        P(None, "tp"),
        P(None, "tp"),
        P(),
        P(),
        P(),
        P(),
        P(),
        P("tp", None),
        P(),
        P("ep", None, "tp"),
        P("ep", None, "tp"),
        P("ep", "tp", None),
    )
    out_specs = (P(("ep", "tp"), None), P("ep", "tp"), P("ep", None, "tp"))
    return jax.shard_map(
        per_device, mesh=mesh, in_specs=in_specs, out_specs=out_specs, check_vma=False
    )
```

profile of v0, /device:TPU:2, one launch (start us, length us, event | category | flops | bytes accessed | tf_op | source)
XLA Modules:
  0.0 219.7 jit_solution(7457263976765336432)
XLA Ops:
  7.2 0.8 convert_element_type.100
  8.0 0.9 fusion.63
  8.9 0.8 fusion.65
  9.8 1.0 broadcast_in_dim.4
  10.8 8.7 %all-to-all-start = ((bf16[16,4,4096]{2,1,0:T(4,128)(2,1)}), bf16[16,4,4096]{2,1,0:T(4,128)(2,1)S(1)}, u32[]{:S(2)}, u32[]{:S(2)}) async-start(bf16[16,4,4096]{2,1,0:T(4,128)(2,1)} %broadcast_in_dim.4), calls=%async_computation | async-start | bytes 1048576 | tf_op jit(solution)/shard_map/all_to_all | solution.py:23
  19.5 0.8 convert_element_type.103
  20.3 0.8 fusion.97
  21.1 0.8 dynamic-slice_convert_fusion.1
  21.8 0.7 dynamic-slice_convert_fusion
  22.5 12.9 %all-to-all-done = bf16[16,4,4096]{2,1,0:T(4,128)(2,1)S(1)} async-done(((bf16[16,4,4096]{2,1,0:T(4,128)(2,1)}), bf16[16,4,4096]{2,1,0:T(4,128)(2,1)S(1)}, u32[]{:S(2)}, u32[]{:S(2)}) %all-to-all-start) | async-done | bytes 524320 | tf_op jit(solution)/shard_map/all_to_all | solution.py:23
  35.6 1.7 fusion.75
  37.3 0.9 fusion.45
  38.2 0.9 fusion.40
  39.2 0.4 multiply_reduce_fusion.1
  39.6 0.3 convolution_convert_fusion.1
  40.3 1.0 pad_maximum_fusion
  41.3 4.2 %all-to-all-start.1 = ((bf16[16,4,4097]{2,1,0:T(4,128)(2,1)}), bf16[16,4,4097]{2,1,0:T(4,128)(2,1)S(1)}, u32[]{:S(2)}, u32[]{:S(2)}) async-start(bf16[16,4,4097]{2,1,0:T(4,128)(2,1)} %pad_maximum_fusion), calls=%async_computation.1 | async-start | bytes 1081344 | tf_op jit(solution)/shard_map/all_to_all | solution.py:39
  46.4 15.6 %all-to-all-done.1 = bf16[16,4,4097]{2,1,0:T(4,128)(2,1)S(1)} async-done(((bf16[16,4,4097]{2,1,0:T(4,128)(2,1)}), bf16[16,4,4097]{2,1,0:T(4,128)(2,1)S(1)}, u32[]{:S(2)}, u32[]{:S(2)}) %all-to-all-start.1) | async-done | bytes 524448 | tf_op jit(solution)/shard_map/all_to_all | solution.py:39
  63.1 15.7 %all_to_all.31 = bf16[16,2,4096]{2,1,0:T(2,128)(2,1)S(1)} all-to-all(bf16[16,2,4096]{2,1,0:T(2,128)(2,1)S(1)} %reshape.224), channel_id=1, replica_groups=mesh['ep'=16,'tp'=16] {'ep'}, dimensions={0} | all-to-all | bytes 524288 | tf_op jit(solution)/shard_map/all_to_all | solution.py:172
  78.8 0.8 all_to_all.25
  79.7 36.6 %all-gather.2.cloned.1.call-done = bf16[1,512,4096]{2,1,0:T(8,128)(2,1)} async-done(((bf16[1,32,4096]{2,1,0:T(8,128)(2,1)}), bf16[1,512,4096]{2,1,0:T(8,128)(2,1)}) %all-gather.2.cloned.1.call-update) | async-done | bytes 4194320 | tf_op jit(solution)/shard_map/all_gather | solution.py:174
  116.3 4.1 %fusion.9 = f32[512,256]{1,0:T(8,128)S(1)} fusion(bf16[1,4096,256]{2,1,0:T(8,128)(2,1)} %param.33, bf16[1,512,4096]{2,1,0:T(8,128)(2,1)} %all-gather.2.cloned.1.call-done), kind=kOutput, calls=%fused_computation.13 | convolution fusion | flops 1073872896 | bytes 6815744 | tf_op jit(solution)/shard_map/erd,edf->erf/dot_general | solution.py:74
  120.4 9.3 %fusion = bf16[1,512,4096]{2,1,0:T(8,128)(2,1)} fusion(bf16[1,256,4096]{2,1,0:T(8,128)(2,1)S(1)} %copy-done, bf16[1,4096,256]{2,1,0:T(8,128)(2,1)} %param.34, bf16[1,512,4096]{2,1,0:T(8,128)(2,1)} %all-gather.2.cloned.1.call-done, f32[512,256]{1,0:T(8,128)S(1)} %fusion.9), kind=kOutput, calls=%fused_computation.1 | convolution fusion | flops 2150760448 | bytes 13107200 | tf_op jit(solution)/shard_map/erf,efd->erd/dot_general | solution.py:80
  129.8 62.0 %reduce-scatter.2.cloned.1.call-done = bf16[1,32,4096]{2,1,0:T(8,128)(2,1)} async-done(((bf16[1,512,4096]{2,1,0:T(8,128)(2,1)}), bf16[1,32,4096]{2,1,0:T(8,128)(2,1)}) %reduce-scatter.2.cloned.1.call-update) | async-done | bytes 262160 | tf_op jit(solution)/shard_map/reduce_scatter | solution.py:176
  191.7 1.5 copy.41
  193.3 0.5 broadcast.161
  193.8 2.2 %reduce.4 = bf16[32,4096]{1,0:T(8,128)(2,1)S(1)} reduce(bf16[32,1,4096]{2,1,0:T(2,128)(2,1)S(1)} %bitcast.111, bf16[]{:T(256)} %broadcast.161), dimensions={1}, to_apply=%bitcast.110.reduce_sub_computation | reduce | bytes 524290
  196.0 0.9 reshape.239
  196.9 7.2 %all-to-all-start.3 = ((bf16[16,2,4096]{2,1,0:T(2,128)(2,1)}), bf16[16,2,4096]{2,1,0:T(2,128)(2,1)S(1)}, u32[]{:S(2)}, u32[]{:S(2)}) async-start(bf16[16,2,4096]{2,1,0:T(2,128)(2,1)} %reshape.239), calls=%async_computation.4 | async-start | bytes 524288 | tf_op jit(solution)/shard_map/all_to_all | solution.py:179
  204.2 0.6 pad_maximum_fusion.1
  204.9 6.6 %all-to-all-done.3 = bf16[16,2,4096]{2,1,0:T(2,128)(2,1)S(1)} async-done(((bf16[16,2,4096]{2,1,0:T(2,128)(2,1)}), bf16[16,2,4096]{2,1,0:T(2,128)(2,1)S(1)}, u32[]{:S(2)}, u32[]{:S(2)}) %all-to-all-start.3) | async-done | bytes 262176 | tf_op jit(solution)/shard_map/all_to_all | solution.py:179
  211.7 1.1 fusion.1
  (47 shorter events, 2.8 us)
Async XLA Ops:
  7.2 113.2 %copy-start = (bf16[1,256,4096]{2,1,0:T(8,128)(2,1)S(1)}, bf16[1,256,4096]{2,1,0:T(8,128)(2,1)}, u32[]{:S(2)}) copy-start(bf16[1,256,4096]{2,1,0:T(8,128)(2,1)} %param.35) | copy-start | bytes 6291460
  10.8 27.4 %copy-start.8 = (f32[64,128]{1,0:T(8,128)S(1)}, f32[64,128]{1,0:T(8,128)}, u32[]{:S(2)}) copy-start(f32[64,128]{1,0:T(8,128)} %param.19) | copy-start | bytes 98308
  10.8 24.6 %all-to-all-start = ((bf16[16,4,4096]{2,1,0:T(4,128)(2,1)}), bf16[16,4,4096]{2,1,0:T(4,128)(2,1)S(1)}, u32[]{:S(2)}, u32[]{:S(2)}) async-start(bf16[16,4,4096]{2,1,0:T(4,128)(2,1)} %broadcast_in_dim.4), calls=%async_computation | async-start | bytes 1048576 | tf_op jit(solution)/shard_map/all_to_all | solution.py:23
  35.6 3.6 %copy-start.1 = (bf16[4096,128]{1,0:T(8,128)(2,1)S(1)}, bf16[4096,128]{1,0:T(8,128)(2,1)}, u32[]{:S(2)}) copy-start(bf16[4096,128]{1,0:T(8,128)(2,1)} %param.25) | copy-start | bytes 3145732
  35.6 4.0 %copy-start.2 = (bf16[128,4096]{1,0:T(8,128)(2,1)S(1)}, bf16[128,4096]{1,0:T(8,128)(2,1)}, u32[]{:S(2)}) copy-start(bf16[128,4096]{1,0:T(8,128)(2,1)} %param.31) | copy-start | bytes 3145732
  39.1 1.0 copy-start.4
  39.6 6.1 %copy-start.7 = (s32[64,4]{0,1:T(4,128)S(1)}, s32[64,4]{0,1:T(4,128)}, u32[]{:S(2)}) copy-start(s32[64,4]{0,1:T(4,128)} %param.21) | copy-start | bytes 3076
  39.6 6.7 %copy-start.5 = (bf16[4096]{0:T(1024)(128)(2,1)S(1)}, bf16[4096]{0:T(1024)(128)(2,1)}, u32[]{:S(2)}) copy-start(bf16[4096]{0:T(1024)(128)(2,1)} %param.32) | copy-start | bytes 24580
  39.9 22.4 %copy-start.3 = (bf16[4,4096]{1,0:T(4,128)(2,1)S(1)}, bf16[4,4096]{1,0:T(4,128)(2,1)}, u32[]{:S(2)}) copy-start(bf16[4,4096]{1,0:T(4,128)(2,1)} %param.18) | copy-start | bytes 98308
  41.3 20.7 %all-to-all-start.1 = ((bf16[16,4,4097]{2,1,0:T(4,128)(2,1)}), bf16[16,4,4097]{2,1,0:T(4,128)(2,1)S(1)}, u32[]{:S(2)}, u32[]{:S(2)}) async-start(bf16[16,4,4097]{2,1,0:T(4,128)(2,1)} %pad_maximum_fusion), calls=%async_computation.1 | async-start | bytes 1081344 | tf_op jit(solution)/shard_map/all_to_all | solution.py:39
  45.6 70.7 %all-gather.2.cloned.1.call-start = ((), (), s32[]{:S(2)}) async-start(), calls=%async_computation.5 | async-start | bytes 4456448 | tf_op jit(solution)/shard_map/all_gather | solution.py:174
  79.6 112.1 %reduce-scatter.2.cloned.1.call-start = ((), (), s32[]{:S(2)}) async-start(), calls=%async_computation.6 | async-start | bytes 4456448 | tf_op jit(solution)/shard_map/reduce_scatter | solution.py:176
  129.8 74.4 %copy-start.6 = (f32[4,4]{1,0:T(4,128)S(1)}, f32[4,4]{1,0:T(4,128)}, u32[]{:S(2)}) copy-start(f32[4,4]{1,0:T(4,128)} %param.22) | copy-start | bytes 196
  129.8 74.5 %slice-start = ((bf16[64,3,128]{2,0,1:T(8,128)(2,1)}), bf16[64,2,128]{2,0,1:T(8,128)(2,1)S(1)}, s32[]{:S(2)}) async-start(bf16[64,3,128]{2,0,1:T(8,128)(2,1)} %param.20), calls=%async_computation.7 | async-start | bytes 65536 | tf_op jit(solution)/shard_map/slice | solution.py:131
  196.9 14.6 %all-to-all-start.3 = ((bf16[16,2,4096]{2,1,0:T(2,128)(2,1)}), bf16[16,2,4096]{2,1,0:T(2,128)(2,1)S(1)}, u32[]{:S(2)}, u32[]{:S(2)}) async-start(bf16[16,2,4096]{2,1,0:T(2,128)(2,1)} %reshape.239), calls=%async_computation.4 | async-start | bytes 524288 | tf_op jit(solution)/shard_map/all_to_all | solution.py:179
Sparse Core Ops, SparseCore 0:
  79.8 36.4 all-gather.1
  129.9 61.8 reduce-scatter.1
where the time goes:
time: 221 us; the launch traced here: 220 us
  waiting for transfers between devices  134 us (61%)
  starting transfers between devices  20.3 us (9%)
  matrix products  19.1 us (9%)
  blocking collectives  15.7 us (7%)
  between operations  14.3 us (6%)
  other arithmetic  10.6 us (5%)
  local copies, waits for them, and re-layouts  5.99 us (3%)
    reduce_scatter x1, waiting for transfers between devices, per_device(): lax.psum_scatter(partials.astype(jnp.bfloat16), 'tp', scatter_dimension=1...  62 us
    all_gather x1, waiting for transfers between devices, per_device(): lax.all_gather(arrived, 'tp', axis=1, tiled=True)  36.6 us
    all_to_all x1, blocking collectives, per_device(): lax.all_to_all(outgoing, 'ep', split_axis=0, concat_axis=1, tiled=True)  15.7 us
    all_to_all x1, waiting for transfers between devices, summed_on_arrival(): tiles = lax.all_to_all(split_up(shard, dim, size), axis, 0, 0, tiled=True)  15.6 us
    all_to_all x1, waiting for transfers between devices, sent_to_all(): lax.all_to_all(jnp.broadcast_to(shard[None], (size, *shard.shape)), axis,...  12.9 us
    dot_general x1, matrix products, run_experts(): jnp.einsum('erf,efd->erd', act, expert_down, preferred_element_type=jnp.f...  9.33 us
    all_to_all x1, starting transfers between devices, sent_to_all(): lax.all_to_all(jnp.broadcast_to(shard[None], (size, *shard.shape)), axis,...  8.7 us
    all_to_all x1, starting transfers between devices, per_device(): lax.all_to_all(summed_rows, 'ep', split_axis=1, concat_axis=0, tiled=True)  7.24 us
  transfers between devices with their start and end apart: 5, of which 5 were waited for; matrix products, arithmetic and copies ran while one was open for 2% of the time, Pallas kernels for 0%

commit v1 on v0

v1 whole, which is shorter than its diff:
```python
import jax
import jax.numpy as jnp
from jax import lax
from jax.experimental import pallas as pl
from jax.experimental.pallas import tpu as pltpu
from jax.sharding import PartitionSpec as P

MESH = pl.DeviceIdType.MESH
BF16, F32, I32 = jnp.bfloat16, jnp.float32, jnp.int32

EPS = 1e-06
CLAMP = 7.0
ALPHA = 1.702
RATE = 8.0

D = 4096
NC = 4
CW = D // NC
TOK = 4
NE = 16
NT = 16
NZ = 8
D_REC = 2048
W = 128
FW = 256
SLOTS = 2
ROWS = NE * SLOTS
HALF = ROWS // 2
TAIL = 128


def iota(shape, dim):
    return lax.broadcasted_iota(I32, shape, dim)


def onehot(cond):
    return jnp.where(cond, 1.0, 0.0).astype(F32)


def dot(a, b):
    return jnp.dot(a, b, preferred_element_type=F32)


def per_token(values):
    part = jnp.broadcast_to(jnp.sum(values, axis=1, keepdims=True), (NC * TOK, 128))
    total = part
    for c in range(1, NC):
        total = total + pltpu.roll(part, c * TOK, 0)
    return total[:, 0:1]


def spread(row_ref):
    c_of = iota((NC * TOK, CW), 0) // TOK
    out = jnp.zeros((NC * TOK, CW), F32)
    for c in range(NC):
        piece = row_ref[:, c * CW : (c + 1) * CW].astype(F32)
        out = jnp.where(c_of == c, jnp.broadcast_to(piece, (NC * TOK, CW)), out)
    return out


def minus_expm1(x):
    small = jnp.full_like(x, 1.0)
    for k in range(8, 1, -1):
        small = 1.0 + small * x * (1.0 / k)
    return jnp.where(x > -0.3, -x * small, 1.0 - jnp.exp(x))


def kernel(
    tokens_ref, rec_ref, conv_ref, ids_ref, weights_ref, gain1_ref, taps_ref, logit_ref, rgain_ref, gain2_ref,
    pin_hbm, pgate_hbm, bdec_hbm, binp_hbm, pout_hbm, eg_hbm, eu_hbm, ed_hbm,
    result_ref, state_ref, newconv_ref,
    wcat, w4, bdec, binp, wgu, wdown,
    tok_s, g1, pb, rp, sb, rb, ob, ib, xg, part, rpart, sums, rright, rleft, ob2, ib2, rw_s,
    lsem, s1, r1, s2p, r2p, s2, r2, s3, r3, s4, r4, s4d, r4d, s5p, r5p, s5, r5r, r5l, s6, r6,
):
    ep = lax.axis_index("ep")
    tp = lax.axis_index("tp")
    z = tp // 2
    core = tp % 2
    other = 1 - core
    mate = (ep, z * 2 + other)

    def along(d):
        return (z + d + NZ) % NZ

    def at_z(zz):
        return (ep, zz * 2 + core)

    barrier = pltpu.get_barrier_semaphore()
    pl.semaphore_signal(barrier, inc=1, device_id=mate, device_id_type=MESH)
    for d in range(1, NZ):
        pl.semaphore_signal(barrier, inc=1, device_id=at_z(along(d)), device_id_type=MESH)
    for d in range(1, NE):
        pl.semaphore_signal(barrier, inc=1, device_id=((ep + d) % NE, tp), device_id_type=MESH)

    loads = [
        pltpu.make_async_copy(pin_hbm, wcat.at[:, pl.ds(0, W)], lsem.at[0]),
        pltpu.make_async_copy(pgate_hbm, wcat.at[:, pl.ds(W, W)], lsem.at[1]),
        pltpu.make_async_copy(bdec_hbm.at[tp], bdec, lsem.at[2]),
        pltpu.make_async_copy(binp_hbm.at[tp], binp, lsem.at[3]),
    ]
    for c in range(NC):
        loads.append(
            pltpu.make_async_copy(
                pout_hbm.at[:, pl.ds(c * CW, CW)], w4.at[pl.ds(c * W, W), :], lsem.at[4 + c]
            )
        )
    loads.append(pltpu.make_async_copy(eg_hbm.at[0], wgu.at[:, pl.ds(0, FW)], lsem.at[8]))
    loads.append(pltpu.make_async_copy(eu_hbm.at[0], wgu.at[:, pl.ds(FW, FW)], lsem.at[9]))
    loads.append(pltpu.make_async_copy(ed_hbm.at[0], wdown, lsem.at[10]))
    for load in loads:
        load.start()

    own = tokens_ref[...].astype(F32)
    for c in range(NC):
        tok_s[c * TOK : (c + 1) * TOK, :] = own[:, c * CW : (c + 1) * CW]
    values = tok_s[...]
    scale = lax.rsqrt(per_token(values * values) * (1.0 / D) + EPS)
    g1[tp] = (values * scale * spread(gain1_ref)).astype(BF16)

    pl.semaphore_wait(barrier, NZ + NE - 1)

    def copy1(dev, slot):
        return pltpu.make_async_remote_copy(
            src_ref=g1.at[slot], dst_ref=g1.at[slot], send_sem=s1, recv_sem=r1.at[slot], device_id=dev, device_id_type=MESH
        )

    for d in (4, 3, 5, 2, 6, 1, 7):
        copy1(at_z(along(d)), tp).start()
    copy1(mate, tp).start()

    q4, r4e = (NC * TOK, W), 8
    row_n, row_c = iota(q4, 0) % TOK, iota(q4, 0) // TOK
    lane_e, lane_c, lane_s = iota(q4, 1) // r4e, (iota(q4, 1) // SLOTS) % NC, iota(q4, 1) % SLOTS
    pick_own = onehot(iota((NC * TOK, NE * TOK), 1) == tp * TOK + iota((NC * TOK, NE * TOK), 0) % TOK)
    own_ids = dot(pick_own.astype(BF16), ids_ref[...].astype(F32).astype(BF16))
    for c in range(NC):
        rw_s[c * TOK : (c + 1) * TOK, :] = weights_ref[...]
    hit = jnp.zeros(q4, F32)
    weighed = jnp.zeros(q4, F32)
    lane_ef = lane_e.astype(F32)
    for k in range(4):
        same = onehot(own_ids[:, k : k + 1] == lane_ef)
        hit = hit + same
        weighed = weighed + same * rw_s[:, k : k + 1]
    sq = (NC * TOK, NC * TOK)
    earlier = onehot(
        (iota(sq, 0) // TOK == iota(sq, 1) // TOK) & (iota(sq, 1) % TOK < iota(sq, 0) % TOK)
    )
    before = dot(earlier.astype(BF16), hit.astype(BF16))
    chosen = hit * onehot((before == lane_s.astype(F32)) & (row_c == lane_c))
    combine = chosen * weighed

    for d in (1, 7, 2, 6, 3, 5, 4):
        slot = along(d) * 2 + core
        copy1(mate, slot).wait_recv()
        copy1(mate, slot).start()
    for d in range(NZ):
        copy1(mate, along(d) * 2 + other).wait_recv()

    big = NT * NC * TOK
    pr, pc = iota((big, big), 0), iota((big, big), 1)
    perm = onehot(pc == ((pr // TOK) % NT) * 16 + (pr // 64) * TOK + pr % TOK).astype(BF16)
    stacked = dot(perm, g1[...].reshape(big, CW)).astype(BF16)
    for load in loads[0:4]:
        load.wait()
    both = jnp.zeros((NT * TOK, 2 * W), F32)
    for c in range(NC):
        both = both + dot(stacked[c * 64 : (c + 1) * 64, :], wcat[c * CW : (c + 1) * CW, :])
    joined = both.astype(BF16)
    branch_in, branch_gate = joined[:, :W].astype(F32), joined[:, W:].astype(F32)

    taps = taps_ref[:, pl.ds(pl.multiple_of(tp * W, W), W)].astype(F32)
    conv = taps[3:4, :] * branch_in
    for tap in range(3):
        conv = conv + taps[tap : tap + 1, :] * conv_ref[:, tap * W : (tap + 1) * W].astype(F32)
    newconv_ref[:, 0 : 2 * W] = conv_ref[:, W : 3 * W]
    newconv_ref[:, 2 * W : 3 * W] = joined[:, :W]

    low = conv.astype(BF16)
    decay_gate = jax.nn.sigmoid(dot(low, bdec[...]))
    input_gate = jax.nn.sigmoid(dot(low, binp[...]))
    mine = iota((NT, W), 0) == tp
    logit = jnp.sum(jnp.where(mine, logit_ref[...], 0.0), axis=0, keepdims=True)
    rgain = jnp.sum(jnp.where(mine, rgain_ref[...].astype(F32), 0.0), axis=0, keepdims=True)
    soft = jnp.maximum(-logit, 0.0) + jnp.log1p(jnp.exp(-jnp.abs(logit)))
    log_keep = -RATE * decay_gate * soft
    new_state = jnp.exp(log_keep) * rec_ref[...] + jnp.sqrt(minus_expm1(2.0 * log_keep)) * input_gate * conv
    state_ref[...] = new_state
    hidden = new_state * jax.nn.gelu(branch_gate)
    squares = jnp.broadcast_to(jnp.sum(hidden * hidden, axis=1, keepdims=True), (NT * TOK, W))

    er, et = iota((big, NT * TOK), 0), iota((big, NT * TOK), 1)
    expand = onehot(et == (((er // 16) % NZ) * 2 + er // 128) * TOK + er % TOK).astype(BF16)
    wide = dot(expand, jnp.concatenate([(hidden * rgain).astype(BF16), squares.astype(BF16)], axis=1))
    gained, sq_wide = wide[:, :W], wide[:, W:]
    c_of = (iota((big, W), 0) // TOK) % NC
    for load in loads[4:8]:
        load.wait()
    lhs = jnp.concatenate([jnp.where(c_of == c, gained, 0.0) for c in range(NC)], axis=1).astype(BF16)
    pb[:, :, :, 0:CW] = dot(lhs, w4[...]).astype(BF16).reshape(2, NZ, 16, CW)
    pb[:, :, :, CW : CW + TAIL] = sq_wide.astype(BF16).reshape(2, NZ, 16, TAIL)

    pair2 = pltpu.make_async_remote_copy(
        src_ref=pb.at[other], dst_ref=rp, send_sem=s2p, recv_sem=r2p, device_id=mate, device_id_type=MESH
    )
    pair2.start()
    pair2.wait_recv()

    def copy2(dev, slot):
        return pltpu.make_async_remote_copy(
            src_ref=sb.at[slot], dst_ref=rb.at[z], send_sem=s2, recv_sem=r2, device_id=dev, device_id_type=MESH
        )

    for d in (4, 3, 5, 2, 6, 1, 7):
        zz = along(d)
        sb[zz] = (pb[core, zz].astype(F32) + rp[zz].astype(F32)).astype(BF16)
        copy2(at_z(zz), zz).start()
    rb[z] = (pb[core, z].astype(F32) + rp[z].astype(F32)).astype(BF16)
    pltpu.make_async_copy(sb.at[pl.ds(0, NZ - 1)], rb.at[pl.ds(0, NZ - 1)], r2).wait()
    summed = jnp.zeros((16, CW + TAIL), F32)
    for zz in range(NZ):
        summed = summed + rb[zz].astype(F32)
    residual = tok_s[...] + summed[:, :CW] * lax.rsqrt(summed[:, CW : CW + 1] * (1.0 / D_REC) + EPS)
    scale = lax.rsqrt(per_token(residual * residual) * (1.0 / D) + EPS)
    second = (residual * scale * spread(gain2_ref)).astype(BF16)
    tok_s[...] = residual

    sent = lax.dot_general(chosen.astype(BF16), second, (((0,), (0,)), ((), ())), preferred_element_type=F32)
    ob[...] = sent.reshape(NE, 8, CW).astype(BF16)
    ib[ep] = ob[ep]

    def copy3(e, src, dst, ss, rs):
        return pltpu.make_async_remote_copy(
            src_ref=src.at[e], dst_ref=dst.at[ep], send_sem=ss, recv_sem=rs, device_id=(e, tp), device_id_type=MESH
        )

    far = (10, 6, 14, 9, 11, 5, 7, 13, 15, 2, 8, 1, 3, 4, 12)
    for d in far:
        copy3((ep + d) % NE, ob, ib, s3, r3).start()
    for load in loads[8:]:
        load.wait()
    pltpu.make_async_copy(ob.at[pl.ds(0, NE - 1)], ib.at[pl.ds(0, NE - 1)], r3).wait()
    own_rows = NE * 8
    sr, sc = iota((own_rows, own_rows), 0), iota((own_rows, own_rows), 1)
    turn = onehot(sc == ((sr // SLOTS) % NE) * 8 + (sr // ROWS) * SLOTS + sr % SLOTS).astype(BF16)
    turned = dot(turn, ib[...].astype(F32).reshape(own_rows, CW).astype(BF16)).astype(BF16)
    for c in range(NC):
        xg[z, core, :, c * CW : (c + 1) * CW] = turned[c * ROWS : (c + 1) * ROWS, :]

    def copy4(zz, h, dev):
        block = xg.at[zz, core, pl.ds(h * HALF, HALF), :]
        return pltpu.make_async_remote_copy(
            src_ref=block, dst_ref=block, send_sem=s4, recv_sem=r4.at[zz * 2 + h], device_id=dev, device_id_type=MESH
        )

    def cross4(zz, h, side):
        block = xg.at[zz, side, pl.ds(h * HALF, HALF), :]
        return pltpu.make_async_remote_copy(
            src_ref=block, dst_ref=block, send_sem=s4d, recv_sem=r4d.at[zz * 2 + h], device_id=mate, device_id_type=MESH
        )

    right, left = at_z(along(1)), at_z(along(-1))
    for h in range(2):
        copy4(z, h, right).start()
        copy4(z, 1 - h, left).start()
    for h in range(2):
        cross4(z, h, core).start()

    def run_expert(zz):
        for h in range(2):
            cross4(zz, h, other).wait_recv()
        rows = xg[zz].reshape(2 * ROWS, D)
        gu = dot(rows, wgu[...])
        gate, up = jnp.minimum(gu[:, :FW], CLAMP), jnp.clip(gu[:, FW:], -CLAMP, CLAMP)
        act = ((up + 1.0) * (gate * jax.nn.sigmoid(ALPHA * gate))).astype(BF16)
        part[zz] = dot(act, wdown[...]).astype(BF16).reshape(2, ROWS, D)
        pltpu.make_async_remote_copy(
            src_ref=part.at[zz, other], dst_ref=rpart.at[zz], send_sem=s5p, recv_sem=r5p.at[zz], device_id=mate, device_id_type=MESH
        ).start()

    for s in range(1, 5):
        for h in range(2):
            for way, hops, nxt in ((-1, 4 - h, right), (1, 3 + h, left)):
                if s <= hops:
                    zz = along(way * s)
                    copy4(zz, h, nxt).wait_recv()
                    if s < hops:
                        copy4(zz, h, nxt).start()
                    cross4(zz, h, core).start()
        if s == 1:
            run_expert(z)
        else:
            pl.loop(0, 2)(lambda i, s=s: run_expert(along((s - 1) * (1 - 2 * i))))
    run_expert(along(4))

    def pair_sum(zz, h):
        rows = slice(h * HALF, (h + 1) * HALF)
        return part[zz, core, rows, :].astype(F32) + rpart[zz, rows, :].astype(F32)

    def wait_pair(zz):
        pltpu.make_async_remote_copy(
            src_ref=part.at[zz, other], dst_ref=rpart.at[zz], send_sem=s5p, recv_sem=r5p.at[zz], device_id=mate, device_id_type=MESH
        ).wait_recv()

    def copy5(zz, h, hop, to_right):
        return pltpu.make_async_remote_copy(
            src_ref=sums.at[zz, h],
            dst_ref=(rright if to_right else rleft).at[h, hop],
            send_sem=s5,
            recv_sem=(r5r if to_right else r5l).at[h * 4 + hop],
            device_id=right if to_right else left,
            device_id_type=MESH,
        )

    def got5(h, hop, from_left):
        return (rright if from_left else rleft)[h, hop].astype(F32)

    for hop in range(4, 0, -1):
        for zz in {4: (along(4),), 3: (along(3), along(-3)), 2: (along(2), along(-2)), 1: (along(1), along(-1))}[hop]:
            wait_pair(zz)
        for h in range(2):
            for to_right, longest in ((True, 4 - h), (False, 3 + h)):
                if hop > longest:
                    continue
                zz = along(hop if to_right else -hop)
                total = pair_sum(zz, h)
                if hop < longest:
                    copy5(zz, h, hop, to_right).wait_recv()
                    total = total + got5(h, hop, to_right)
                sums[zz, h] = total.astype(BF16)
                copy5(zz, h, hop - 1, to_right).start()
    wait_pair(z)
    for h in range(2):
        total = pair_sum(z, h)
        for to_right in (True, False):
            copy5(z, h, 0, to_right).wait_recv()
            total = total + got5(h, 0, to_right)
        sums[z, h] = total.astype(BF16)

    mine = jnp.concatenate([sums[z].reshape(ROWS, D)[:, c * CW : (c + 1) * CW] for c in range(NC)], axis=0)
    back = onehot(sr == ((sc // SLOTS) % NE) * 8 + (sc // ROWS) * SLOTS + sc % SLOTS).astype(BF16)
    ob2[...] = dot(back, mine).reshape(NE, 8, CW).astype(BF16)
    ib2[ep] = ob2[ep]
    for d in far:
        copy3((ep + d) % NE, ob2, ib2, s6, r6).start()
    high = combine.astype(BF16)
    rest = combine - high.astype(F32)
    middle = rest.astype(BF16)
    lowest = (rest - middle.astype(F32)).astype(BF16)
    pltpu.make_async_copy(ob2.at[pl.ds(0, NE - 1)], ib2.at[pl.ds(0, NE - 1)], r6).wait()
    returned = ib2[...].astype(F32).reshape(NE * 8, CW).astype(BF16)
    mix = dot(lowest, returned) + dot(middle, returned) + dot(high, returned)
    tok_s[...] = tok_s[...] + mix
    for c in range(NC):
        result_ref[:, c * CW : (c + 1) * CW] = tok_s[c * TOK : (c + 1) * TOK, :].astype(BF16)

    def drain(ref, sem):
        pltpu.make_async_copy(ref, ref, sem).wait()

    drain(g1.at[pl.ds(0, NT - 1)], s1)
    pair2.wait_send()
    drain(sb.at[pl.ds(0, NZ - 1)], s2)
    drain(ob.at[pl.ds(0, NE - 1)], s3)
    drain(xg.at[pl.ds(0, NZ - 1), 0], s4)
    drain(xg.at[:, 0], s4d)
    drain(rpart, s5p)
    drain(sums.at[pl.ds(0, NZ - 1)], s5)
    drain(ob2.at[pl.ds(0, NE - 1)], s6)


def per_device(
    tokens, rec_state, conv_state, route_ids, route_weights, first_gain, proj_input, proj_gate, conv_taps,
    decay_logit, block_decay, block_input, rec_gain, proj_out, second_gain, expert_gate, expert_up, expert_down,
):
    seqs = rec_state.shape[0]
    vmem, hbm = pl.BlockSpec(memory_space=pltpu.VMEM), pl.BlockSpec(memory_space=pl.ANY)
    dma, v = pltpu.SemaphoreType.DMA, pltpu.VMEM
    result, new_state, new_conv = pl.pallas_call(
        kernel,
        name="layer",
        out_shape=(
            jax.ShapeDtypeStruct(tokens.shape, BF16),
            jax.ShapeDtypeStruct(rec_state.shape, F32),
            jax.ShapeDtypeStruct((seqs, 3 * W), BF16),
        ),
        in_specs=[vmem] * 10 + [hbm] * 8,
        out_specs=(vmem, vmem, vmem),
        scratch_shapes=[
            v((D, 2 * W), BF16), v((NC * W, CW), BF16), v((W, W), BF16), v((W, W), BF16),
            v((D, 2 * FW), BF16), v((FW, D), BF16),
            v((16, CW), F32), v((NT, 16, CW), BF16),
            v((2, NZ, 16, CW + TAIL), BF16), v((NZ, 16, CW + TAIL), BF16), v((NZ, 16, CW + TAIL), BF16),
            v((NZ, 16, CW + TAIL), BF16),
            v((NE, 8, CW), BF16), v((NE, 8, CW), BF16),
            v((NZ, 2, ROWS, D), BF16), v((NZ, 2, ROWS, D), BF16), v((NZ, ROWS, D), BF16),
            v((NZ, 2, HALF, D), BF16), v((2, 4, HALF, D), BF16), v((2, 4, HALF, D), BF16),
            v((NE, 8, CW), BF16), v((NE, 8, CW), BF16), v((16, 4), F32),
            dma((11,)), dma, dma((NT,)), dma, dma, dma, dma, dma, dma,
            dma, dma((NZ * 2,)), dma, dma((NZ * 2,)), dma, dma((NZ,)), dma, dma((8,)), dma((8,)), dma, dma,
        ],
        compiler_params=pltpu.CompilerParams(
            collective_id=0, has_side_effects=True, vmem_limit_bytes=60 * 1024 * 1024
        ),
    )(
        tokens, rec_state, conv_state.reshape(seqs, 3 * W), route_ids, route_weights, first_gain.reshape(1, D),
        conv_taps, decay_logit.reshape(NT, W), rec_gain.reshape(NT, W), second_gain.reshape(1, D),
        proj_input, proj_gate, block_decay, block_input, proj_out, expert_gate, expert_up, expert_down,
    )
    return result, new_state, new_conv.reshape(seqs, 3, W)


def solution(mesh):
    in_specs = (
        P(("ep", "tp"), None),
        P("ep", "tp"),
        P("ep", None, "tp"),
        P("ep", None),
        P(("ep", "tp"), None),
        P(),
        P(None, "tp"),
        P(None, "tp"),
        P(),
        P(),
        P(),
        P(),
        P(),
        P("tp", None),
        P(),
        P("ep", None, "tp"),
        P("ep", None, "tp"),
        P("ep", "tp", None),
    )
    out_specs = (P(("ep", "tp"), None), P("ep", "tp"), P("ep", None, "tp"))
    return jax.shard_map(
        per_device, mesh=mesh, in_specs=in_specs, out_specs=out_specs, check_vma=False
    )
```

time: 221 us -> 108 us (0.49)
  waiting for transfers between devices: 134 us -> 0 us
  Pallas kernels: 0 us -> 96.9 us
  starting transfers between devices: 20.3 us -> 0 us
  matrix products: 19.1 us -> 0 us
  blocking collectives: 15.7 us -> 0 us
  between operations: 14.3 us -> 0.65 us
  other arithmetic: 10.6 us -> 0 us
  local copies, waits for them, and re-layouts: 5.99 us -> 8.83 us
    pallas_call x0 -> x1, Pallas kernels: none -> 96.9 us  [per_device(): pl.pallas_call(kernel, name='layer', out_shape=(jax.ShapeDtypeStruct(toke...]
    reduce_scatter x1 -> x0, waiting for transfers between devices: 62 us -> none  [per_device(): lax.psum_scatter(partials.astype(jnp.bfloat16), 'tp', scatter_dimension=1...]
    all_gather x1 -> x0, waiting for transfers between devices: 36.6 us -> none  [per_device(): lax.all_gather(arrived, 'tp', axis=1, tiled=True)]
    all_to_all x3 -> x0, waiting for transfers between devices: 35.1 us -> none  [the longest x1 15.6 us: summed_on_arrival(): tiles = lax.all_to_all(split_up(shard, dim, size), axis, 0, 0, tiled=True)]
    all_to_all x3 -> x0, starting transfers between devices: 20.2 us -> none  [the longest x1 8.7 us: sent_to_all(): lax.all_to_all(jnp.broadcast_to(shard[None], (size, *shard.shape)), axis,...]
    dot_general x9 -> x0, matrix products: 19.1 us -> none  [the longest x1 9.33 us: run_experts(): jnp.einsum('erf,efd->erd', act, expert_down, preferred_element_type=jnp.f...]
    all_to_all x1 -> x0, blocking collectives: 15.7 us -> none  [per_device(): lax.all_to_all(outgoing, 'ep', split_axis=0, concat_axis=1, tiled=True)]
    convert_element_type x7 -> x0, other arithmetic: 4.03 us -> none  [the longest x2 0.85 us: norm_rows(): return values * scale * gain.astype(jnp.float32)]
  transfers between devices with their start and end apart: 5 -> 0, of which waited for: 5 -> 0; matrix products, arithmetic and copies ran while one was open for 2% -> 0% of each run, Pallas kernels for 0% -> 0%
where the time goes in v1:
time: 108 us; the launch traced here: 106 us
  Pallas kernels  96.9 us (90%)
  local copies, waits for them, and re-layouts  8.83 us (8%)
    pallas_call x1, Pallas kernels, per_device(): pl.pallas_call(kernel, name='layer', out_shape=(jax.ShapeDtypeStruct(toke...  96.9 us
    unnamed x6, local copies, waits for them, and re-layouts  5.58 us

profile of v1, /device:TPU:2, one launch (start us, length us, event | category | flops | bytes accessed | tf_op | source)
XLA Modules:
  0.0 106.4 jit_solution(1570929115039717405)
XLA Ops:
  0.6 0.0 copy-start
  0.6 1.3 %reshape.25.gain1_ref = bf16[1,4096]{1,0:T(2,128)(2,1)} reshape(bf16[4096]{0:T(1024)(128)(2,1)} %param.23) | data formatting | bytes 16384 | tf_op jit(solution)/shard_map/reshape | solution.py:406
  2.0 1.3 %reshape.28.gain2_ref = bf16[1,4096]{1,0:T(2,128)(2,1)} reshape(bf16[4096]{0:T(1024)(128)(2,1)} %param.32) | data formatting | bytes 16384 | tf_op jit(solution)/shard_map/reshape | solution.py:407
  3.3 1.4 %copy.25.ids_ref = s32[64,4]{1,0:T(8,128)} copy(s32[64,4]{0,1:T(4,128)} %param.21) | data formatting | bytes 2048 | tf_op args[3]
  4.7 0.0 copy-done
  4.7 0.6 copy_bitcast_fusion.conv_ref
  5.3 96.9 %layer.1 = (bf16[4,4096]{1,0:T(4,128)(2,1)}, f32[64,128]{1,0:T(8,128)}, bf16[64,384]{1,0:T(8,128)(2,1)}) custom-call(bf16[4,4096]{1,0:T(4,128)(2,1)} %tokens_ref.1, f32[64,128]{1,0:T(8,128)} %rec_ref.1, bf16[64,384]{1,0:T(8,128)(2,1)} %copy_bitcast_fusion.conv_ref, s32[64,4]{1,0:T(8,128)} %copy.25.ids_ref, f32[4,4]{1,0:T(4,128)} %weights_ref.1, ...), custom_call_target="tpu_custom_call" | custom-call | tf_op jit(solution)/shard_map/layer/pallas_call | solution.py:379
  102.2 1.4 %copy_bitcast_fusion.1 = bf16[64,3,128]{2,0,1:T(8,128)(2,1)} fusion(bf16[64,384]{1,0:T(8,128)(2,1)} %get-tuple-element.8), kind=kLoop, calls=%fused_computation.1 | loop fusion | bytes 98304
  103.7 1.4 %copy.33 = bf16[4,4096]{1,0:T(4,128)(2,1)} copy(bf16[4,4096]{1,0:T(4,128)(2,1)} %get-tuple-element.18) | data formatting | bytes 65536
  105.1 1.4 %copy.34 = f32[64,128]{1,0:T(8,128)} copy(f32[64,128]{1,0:T(8,128)} %get-tuple-element.19) | data formatting | bytes 65536
Async XLA Ops:
  0.6 4.0 %copy-start = (bf16[64,3,128]{2,0,1:T(8,128)(2,1)S(1)}, bf16[64,3,128]{2,0,1:T(8,128)(2,1)}, u32[]{:S(2)}) copy-start(bf16[64,3,128]{2,0,1:T(8,128)(2,1)} %param.20) | copy-start | bytes 147460

commit v2 on v1

--- a/solution.py
+++ b/solution.py
@@ -49,13 +49,17 @@
     return total[:, 0:1]
 
 
-def spread(row_ref):
-    c_of = iota((NC * TOK, CW), 0) // TOK
-    out = jnp.zeros((NC * TOK, CW), F32)
-    for c in range(NC):
-        piece = row_ref[:, c * CW : (c + 1) * CW].astype(F32)
-        out = jnp.where(c_of == c, jnp.broadcast_to(piece, (NC * TOK, CW)), out)
-    return out
+def spread(ref):
+    values, shape = ref[...].astype(F32), (NC * TOK, 128)
+    c_of = iota(shape, 0) // TOK
+    blocks = []
+    for i in range(CW // 128):
+        block = jnp.broadcast_to(values[i : i + 1, :], shape)
+        for c in range(1, NC):
+            row = c * (CW // 128) + i
+            block = jnp.where(c_of == c, jnp.broadcast_to(values[row : row + 1, :], shape), block)
+        blocks.append(block)
+    return jnp.concatenate(blocks, axis=1)
 
 
 def minus_expm1(x):
@@ -66,9 +70,10 @@
 
 
 def kernel(
-    tokens_ref, rec_ref, conv_ref, ids_ref, weights_ref, gain1_ref, taps_ref, logit_ref, rgain_ref, gain2_ref,
+    tokens_hbm, gain1_hbm, ids_hbm, weights_hbm, rec_hbm, conv_hbm, logit_hbm, rgain_hbm, gain2_hbm, taps_hbm,
     pin_hbm, pgate_hbm, bdec_hbm, binp_hbm, pout_hbm, eg_hbm, eu_hbm, ed_hbm,
     result_ref, state_ref, newconv_ref,
+    tokens_ref, gain1_ref, ids_ref, weights_ref, rec_ref, conv_ref, logit_ref, rgain_ref, gain2_ref, taps_ref,
     wcat, w4, bdec, binp, wgu, wdown,
     tok_s, g1, pb, rp, sb, rb, ob, ib, xg, part, rpart, sums, rright, rleft, ob2, ib2, rw_s,
     lsem, s1, r1, s2p, r2p, s2, r2, s3, r3, s4, r4, s4d, r4d, s5p, r5p, s5, r5r, r5l, s6, r6,
@@ -93,6 +98,16 @@
     for d in range(1, NE):
         pl.semaphore_signal(barrier, inc=1, device_id=((ep + d) % NE, tp), device_id_type=MESH)
 
+    smalls = [
+        pltpu.make_async_copy(src, dst, lsem.at[11 + i])
+        for i, (src, dst) in enumerate((
+            (tokens_hbm, tokens_ref), (gain1_hbm, gain1_ref), (ids_hbm, ids_ref), (weights_hbm, weights_ref),
+            (rec_hbm, rec_ref), (conv_hbm, conv_ref), (logit_hbm, logit_ref), (rgain_hbm, rgain_ref),
+            (gain2_hbm, gain2_ref), (taps_hbm.at[:, pl.ds(pl.multiple_of(tp * W, W), W)], taps_ref),
+        ))
+    ]
+    for load in smalls:
+        load.start()
     loads = [
         pltpu.make_async_copy(pin_hbm, wcat.at[:, pl.ds(0, W)], lsem.at[0]),
         pltpu.make_async_copy(pgate_hbm, wcat.at[:, pl.ds(W, W)], lsem.at[1]),
@@ -111,6 +126,8 @@
     for load in loads:
         load.start()
 
+    smalls[0].wait()
+    smalls[1].wait()
     own = tokens_ref[...].astype(F32)
     for c in range(NC):
         tok_s[c * TOK : (c + 1) * TOK, :] = own[:, c * CW : (c + 1) * CW]
@@ -133,7 +150,10 @@
     row_n, row_c = iota(q4, 0) % TOK, iota(q4, 0) // TOK
     lane_e, lane_c, lane_s = iota(q4, 1) // r4e, (iota(q4, 1) // SLOTS) % NC, iota(q4, 1) % SLOTS
     pick_own = onehot(iota((NC * TOK, NE * TOK), 1) == tp * TOK + iota((NC * TOK, NE * TOK), 0) % TOK)
-    own_ids = dot(pick_own.astype(BF16), ids_ref[...].astype(F32).astype(BF16))
+    smalls[2].wait()
+    smalls[3].wait()
+    all_ids = ids_ref[...].astype(F32).astype(BF16)
+    own_ids = lax.dot_general(pick_own.astype(BF16), all_ids, (((1,), (1,)), ((), ())), preferred_element_type=F32)
     for c in range(NC):
         rw_s[c * TOK : (c + 1) * TOK, :] = weights_ref[...]
     hit = jnp.zeros(q4, F32)
@@ -162,7 +182,7 @@
     pr, pc = iota((big, big), 0), iota((big, big), 1)
     perm = onehot(pc == ((pr // TOK) % NT) * 16 + (pr // 64) * TOK + pr % TOK).astype(BF16)
     stacked = dot(perm, g1[...].reshape(big, CW)).astype(BF16)
-    for load in loads[0:4]:
+    for load in loads[0:4] + smalls[4:]:
         load.wait()
     both = jnp.zeros((NT * TOK, 2 * W), F32)
     for c in range(NC):
@@ -170,12 +190,12 @@
     joined = both.astype(BF16)
     branch_in, branch_gate = joined[:, :W].astype(F32), joined[:, W:].astype(F32)
 
-    taps = taps_ref[:, pl.ds(pl.multiple_of(tp * W, W), W)].astype(F32)
+    taps = taps_ref[...].astype(F32)
     conv = taps[3:4, :] * branch_in
     for tap in range(3):
-        conv = conv + taps[tap : tap + 1, :] * conv_ref[:, tap * W : (tap + 1) * W].astype(F32)
-    newconv_ref[:, 0 : 2 * W] = conv_ref[:, W : 3 * W]
-    newconv_ref[:, 2 * W : 3 * W] = joined[:, :W]
+        conv = conv + taps[tap : tap + 1, :] * conv_ref[tap].astype(F32)
+    newconv_ref[0:2] = conv_ref[1:3]
+    newconv_ref[2] = joined[:, :W]
 
     low = conv.astype(BF16)
     decay_gate = jax.nn.sigmoid(dot(low, bdec[...]))
@@ -264,8 +284,8 @@
     for h in range(2):
         copy4(z, h, right).start()
         copy4(z, 1 - h, left).start()
-    for h in range(2):
-        cross4(z, h, core).start()
+    cross4(z, 0, core).start()
+    cross4(z, 1, core).start()
 
     def run_expert(zz):
         for h in range(2):
@@ -280,8 +300,8 @@
         ).start()
 
     for s in range(1, 5):
-        for h in range(2):
-            for way, hops, nxt in ((-1, 4 - h, right), (1, 3 + h, left)):
+        for i in range(2):
+            for h, way, hops, nxt in ((i, -1, 4 - i, right), (1 - i, 1, 4 - i, left)):
                 if s <= hops:
                     zz = along(way * s)
                     copy4(zz, h, nxt).wait_recv()
@@ -292,8 +312,6 @@
             run_expert(z)
         else:
             pl.loop(0, 2)(lambda i, s=s: run_expert(along((s - 1) * (1 - 2 * i))))
-    run_expert(along(4))
-
     def pair_sum(zz, h):
         rows = slice(h * HALF, (h + 1) * HALF)
         return part[zz, core, rows, :].astype(F32) + rpart[zz, rows, :].astype(F32)
@@ -316,20 +334,35 @@
     def got5(h, hop, from_left):
         return (rright if from_left else rleft)[h, hop].astype(F32)
 
-    for hop in range(4, 0, -1):
-        for zz in {4: (along(4),), 3: (along(3), along(-3)), 2: (along(2), along(-2)), 1: (along(1), along(-1))}[hop]:
-            wait_pair(zz)
-        for h in range(2):
-            for to_right, longest in ((True, 4 - h), (False, 3 + h)):
-                if hop > longest:
-                    continue
-                zz = along(hop if to_right else -hop)
-                total = pair_sum(zz, h)
-                if hop < longest:
-                    copy5(zz, h, hop, to_right).wait_recv()
-                    total = total + got5(h, hop, to_right)
-                sums[zz, h] = total.astype(BF16)
-                copy5(zz, h, hop - 1, to_right).start()
+    def pass_on(hop, h, to_right):
+        zz = along(hop if to_right else -hop)
+        total = pair_sum(zz, h)
+        if hop < (4 - h if to_right else 3 + h):
+            copy5(zz, h, hop, to_right).wait_recv()
+            total = total + got5(h, hop, to_right)
+        sums[zz, h] = total.astype(BF16)
+        copy5(zz, h, hop - 1, to_right).start()
+
+    wait_pair(along(3))
+    pass_on(3, 1, True)
+    wait_pair(along(-3))
+    pass_on(3, 0, False)
+    run_expert(along(4))
+    wait_pair(along(2))
+    wait_pair(along(-2))
+    wait_pair(along(4))
+    pass_on(4, 0, True)
+    pass_on(4, 1, False)
+    for hop in (2, 1):
+        pass_on(hop, 1, True)
+        pass_on(hop, 0, False)
+        if hop == 2:
+            wait_pair(along(1))
+            wait_pair(along(-1))
+        pass_on(hop + 1, 0, True)
+        pass_on(hop + 1, 1, False)
+    pass_on(1, 0, True)
+    pass_on(1, 1, False)
     wait_pair(z)
     for h in range(2):
         total = pair_sum(z, h)
@@ -379,14 +412,12 @@
     result, new_state, new_conv = pl.pallas_call(
         kernel,
         name="layer",
-        out_shape=(
-            jax.ShapeDtypeStruct(tokens.shape, BF16),
-            jax.ShapeDtypeStruct(rec_state.shape, F32),
-            jax.ShapeDtypeStruct((seqs, 3 * W), BF16),
-        ),
-        in_specs=[vmem] * 10 + [hbm] * 8,
+        out_shape=(v(tokens.shape, BF16), v(rec_state.shape, F32), v((3, seqs, W), BF16)),
+        in_specs=[hbm] * 18,
         out_specs=(vmem, vmem, vmem),
         scratch_shapes=[
+            v(tokens.shape, BF16), v((D // W, W), BF16), v((TOK, seqs), I32), v((TOK, TOK), F32),
+            v((seqs, W), F32), v((3, seqs, W), BF16), v((NT, W), F32), v((NT, W), BF16), v((D // W, W), BF16), v((TOK, W), BF16),
             v((D, 2 * W), BF16), v((NC * W, CW), BF16), v((W, W), BF16), v((W, W), BF16),
             v((D, 2 * FW), BF16), v((FW, D), BF16),
             v((16, CW), F32), v((NT, 16, CW), BF16),
@@ -396,18 +427,18 @@
             v((NZ, 2, ROWS, D), BF16), v((NZ, 2, ROWS, D), BF16), v((NZ, ROWS, D), BF16),
             v((NZ, 2, HALF, D), BF16), v((2, 4, HALF, D), BF16), v((2, 4, HALF, D), BF16),
             v((NE, 8, CW), BF16), v((NE, 8, CW), BF16), v((16, 4), F32),
-            dma((11,)), dma, dma((NT,)), dma, dma, dma, dma, dma, dma,
+            dma((21,)), dma, dma((NT,)), dma, dma, dma, dma, dma, dma,
             dma, dma((NZ * 2,)), dma, dma((NZ * 2,)), dma, dma((NZ,)), dma, dma((8,)), dma((8,)), dma, dma,
         ],
         compiler_params=pltpu.CompilerParams(
             collective_id=0, has_side_effects=True, vmem_limit_bytes=60 * 1024 * 1024
         ),
     )(
-        tokens, rec_state, conv_state.reshape(seqs, 3 * W), route_ids, route_weights, first_gain.reshape(1, D),
-        conv_taps, decay_logit.reshape(NT, W), rec_gain.reshape(NT, W), second_gain.reshape(1, D),
+        tokens, first_gain.reshape(D // W, W), route_ids.T, route_weights, rec_state, conv_state.transpose(1, 0, 2),
+        decay_logit.reshape(NT, W), rec_gain.reshape(NT, W), second_gain.reshape(D // W, W), conv_taps,
         proj_input, proj_gate, block_decay, block_input, proj_out, expert_gate, expert_up, expert_down,
     )
-    return result, new_state, new_conv.reshape(seqs, 3, W)
+    return result, new_state, new_conv.transpose(1, 0, 2)
 
 
 def solution(mesh):

time: 108 us -> 94.6 us (0.88); the launches traced: 106 us -> 94.5 us
  local copies, waits for them, and re-layouts: 8.83 us -> 1.85 us
  Pallas kernels: 96.9 us -> 92 us
    pallas_call x1, Pallas kernels: 96.9 us -> 92 us  [per_device(): pl.pallas_call(kernel, name='layer', out_shape=(v(tokens.shape, BF16), v(...]
    unnamed x6 -> x3, local copies, waits for them, and re-layouts: 5.58 us -> 1.85 us
    reshape x3 -> x0, local copies, waits for them, and re-layouts: 3.25 us -> none  [the longest x1 1.32 us: per_device(): first_gain.reshape(1, D)]
where the time goes in v2:
time: 94.6 us; the launch traced here: 94.5 us
  Pallas kernels  92 us (97%)
  local copies, waits for them, and re-layouts  1.85 us (2%)
    pallas_call x1, Pallas kernels, per_device(): pl.pallas_call(kernel, name='layer', out_shape=(v(tokens.shape, BF16), v(...  92 us

profile of v2, /device:TPU:2, one launch (start us, length us, event | category | flops | bytes accessed | tf_op | source)
XLA Modules:
  0.0 94.5 jit_solution(5210472051071129678)
XLA Ops:
  0.6 92.0 %layer.1 = (bf16[4,4096]{1,0:T(4,128)(2,1)S(1)}, f32[64,128]{1,0:T(8,128)S(1)}, bf16[3,64,128]{2,1,0:T(8,128)(2,1)S(1)}) custom-call(bf16[4,4096]{1,0:T(4,128)(2,1)} %tokens_hbm.1, bf16[32,128]{1,0:T(8,128)(2,1)} %bitcast.9, s32[4,64]{1,0:T(4,128)} %bitcast.13, f32[4,4]{1,0:T(4,128)} %weights_hbm.1, f32[64,128]{1,0:T(8,128)} %rec_hbm.1, ...), custom_call_target="tpu_custom_call" | custom-call | tf_op jit(solution)/shard_map/layer/pallas_call | solution.py:412
  92.6 0.6 copy.24
  93.3 0.6 copy.25
  93.9 0.6 copy.26

commit v3 on v2

--- a/solution.py
+++ b/solution.py
@@ -27,6 +27,9 @@
 ROWS = NE * SLOTS
 HALF = ROWS // 2
 TAIL = 128
+CB = 384
+CA = CW - CB
+DA, DB = NC * CA, NC * CB
 
 
 def iota(shape, dim):
@@ -74,9 +77,11 @@
     pin_hbm, pgate_hbm, bdec_hbm, binp_hbm, pout_hbm, eg_hbm, eu_hbm, ed_hbm,
     result_ref, state_ref, newconv_ref,
     tokens_ref, gain1_ref, ids_ref, weights_ref, rec_ref, conv_ref, logit_ref, rgain_ref, gain2_ref, taps_ref,
-    wcat, w4, bdec, binp, wgu, wdown,
-    tok_s, g1, pb, rp, sb, rb, ob, ib, xg, part, rpart, sums, rright, rleft, ob2, ib2, rw_s,
+    wcat, w4, bdec, binp, wgu_a, wgu_b, wdown_a, wdown_b,
+    tok_s, g1, pb, rp, sb, rb, ob, ib, xa, acc, part_a, rpart_a, sums, rright, rleft, ob2, ib2, rw_s,
+    sg, tb, xr, xb, part_b, rpart_b, tb2, rr, cb, rcb,
     lsem, s1, r1, s2p, r2p, s2, r2, s3, r3, s4, r4, s4d, r4d, s5p, r5p, s5, r5r, r5l, s6, r6,
+    sb1, rb1, sb2, rb2, sb2d, rb2d, sbp, rbp, sb3, rb3, sb4, rb4,
 ):
     ep = lax.axis_index("ep")
     tp = lax.axis_index("tp")
@@ -84,6 +89,15 @@
     core = tp % 2
     other = 1 - core
     mate = (ep, z * 2 + other)
+    y, x = ep // 4, ep % 4
+
+    def remote(src, dst, ss, rs, dev):
+        return pltpu.make_async_remote_copy(
+            src_ref=src, dst_ref=dst, send_sem=ss, recv_sem=rs, device_id=dev, device_id_type=MESH
+        )
+
+    def over(dy, dx):
+        return ((y + dy + 4) % 4) * 4 + (x + dx + 4) % 4
 
     def along(d):
         return (z + d + NZ) % NZ
@@ -120,11 +134,20 @@
                 pout_hbm.at[:, pl.ds(c * CW, CW)], w4.at[pl.ds(c * W, W), :], lsem.at[4 + c]
             )
         )
-    loads.append(pltpu.make_async_copy(eg_hbm.at[0], wgu.at[:, pl.ds(0, FW)], lsem.at[8]))
-    loads.append(pltpu.make_async_copy(eu_hbm.at[0], wgu.at[:, pl.ds(FW, FW)], lsem.at[9]))
-    loads.append(pltpu.make_async_copy(ed_hbm.at[0], wdown, lsem.at[10]))
     for load in loads:
         load.start()
+    for c in range(NC):
+        for i, (hbm, col) in enumerate(((eg_hbm, 0), (eu_hbm, FW))):
+            for dst, first, size, sem in ((wgu_a, 0, CA, 8), (wgu_b, CA, CB, 9)):
+                pltpu.make_async_copy(
+                    hbm.at[0, pl.ds(c * CW + first, size), :],
+                    dst.at[pl.ds(c * size, size), pl.ds(col, FW)],
+                    lsem.at[sem],
+                ).start()
+        for dst, first, size, sem in ((wdown_a, 0, CA, 10), (wdown_b, CA, CB, 21)):
+            pltpu.make_async_copy(
+                ed_hbm.at[0, :, pl.ds(c * CW + first, size)], dst.at[:, pl.ds(c * size, size)], lsem.at[sem]
+            ).start()
 
     smalls[0].wait()
     smalls[1].wait()
@@ -170,6 +193,26 @@
     before = dot(earlier.astype(BF16), hit.astype(BF16))
     chosen = hit * onehot((before == lane_s.astype(F32)) & (row_c == lane_c))
     combine = chosen * weighed
+
+    qn, rn = NZ * NC * TOK, NE * NZ * SLOTS
+    big_q = (qn, rn)
+    pick_core = onehot(
+        iota((qn, NE * TOK), 1) == ((iota((qn, NE * TOK), 0) // 16) * 2 + core) * TOK + iota((qn, NE * TOK), 0) % TOK
+    )
+    core_ids = lax.dot_general(pick_core.astype(BF16), all_ids, (((1,), (1,)), ((), ())), preferred_element_type=F32)
+    big_e = (iota(big_q, 1) // (NZ * SLOTS)).astype(F32)
+    big_s = (iota(big_q, 1) % SLOTS).astype(F32)
+    same_z = iota(big_q, 0) // 16 == (iota(big_q, 1) // SLOTS) % NZ
+    big_hit = jnp.zeros(big_q, F32)
+    for k in range(4):
+        big_hit = big_hit + onehot(core_ids[:, k : k + 1] == big_e)
+    qq = (qn, qn)
+    big_earlier = onehot(
+        (iota(qq, 0) // TOK == iota(qq, 1) // TOK) & (iota(qq, 1) % TOK < iota(qq, 0) % TOK)
+    )
+    big_before = dot(big_earlier.astype(BF16), big_hit.astype(BF16))
+    big_chosen = big_hit * onehot((big_before == big_s) & same_z)
+    c_of_q = (iota(big_q, 0) // TOK) % NC
 
     for d in (1, 7, 2, 6, 3, 5, 4):
         slot = along(d) * 2 + core
@@ -246,39 +289,53 @@
     second = (residual * scale * spread(gain2_ref)).astype(BF16)
     tok_s[...] = residual
 
-    sent = lax.dot_general(chosen.astype(BF16), second, (((0,), (0,)), ((), ())), preferred_element_type=F32)
-    ob[...] = sent.reshape(NE, 8, CW).astype(BF16)
+    w_high = rw_s[...].astype(BF16).astype(F32)
+    w_rest = rw_s[...] - w_high
+    lane = iota((NC * TOK, TAIL), 1)
+    tail = jnp.zeros((NC * TOK, TAIL), F32)
+    for k in range(4):
+        tail = jnp.where(lane == k, w_high[:, k : k + 1], tail)
+        tail = jnp.where(lane == 4 + k, w_rest[:, k : k + 1], tail)
+    sg[z, :, 0:CB] = second[:, CA:]
+    sg[z, :, CB:] = tail.astype(BF16)
+    sent = lax.dot_general(
+        chosen.astype(BF16), second[:, :CA], (((0,), (0,)), ((), ())), preferred_element_type=F32
+    )
+    ob[...] = sent.reshape(NE, 8, CA).astype(BF16)
     ib[ep] = ob[ep]
-
-    def copy3(e, src, dst, ss, rs):
-        return pltpu.make_async_remote_copy(
-            src_ref=src.at[e], dst_ref=dst.at[ep], send_sem=ss, recv_sem=rs, device_id=(e, tp), device_id_type=MESH
-        )
-
-    far = (10, 6, 14, 9, 11, 5, 7, 13, 15, 2, 8, 1, 3, 4, 12)
-    for d in far:
-        copy3((ep + d) % NE, ob, ib, s3, r3).start()
-    for load in loads[8:]:
-        load.wait()
-    pltpu.make_async_copy(ob.at[pl.ds(0, NE - 1)], ib.at[pl.ds(0, NE - 1)], r3).wait()
+    for d in (4, 3, 5, 2, 6, 1, 7):
+        remote(sg.at[z], sg.at[z], sb1, rb1, at_z(along(d))).start()
+
+    ways = (
+        (2, 2), (2, 1), (1, 3), (3, 2), (0, 2), (2, 3), (1, 2), (2, 0),
+        (3, 1), (3, 3), (1, 1), (0, 3), (1, 0), (0, 1), (3, 0),
+    )
+
+    def to_experts(src, dst, ss, rs):
+        for dy, dx in ways:
+            e = over(dy, dx)
+            remote(src.at[e], dst.at[ep], ss, rs, (e, tp)).start()
+
+    to_experts(ob, ib, s3, r3)
+
+    def all_of(ref, sem):
+        pltpu.make_async_copy(ref, ref, sem).wait()
+
+    all_of(ib.at[pl.ds(0, NE - 1)], r3)
     own_rows = NE * 8
     sr, sc = iota((own_rows, own_rows), 0), iota((own_rows, own_rows), 1)
     turn = onehot(sc == ((sr // SLOTS) % NE) * 8 + (sr // ROWS) * SLOTS + sr % SLOTS).astype(BF16)
-    turned = dot(turn, ib[...].astype(F32).reshape(own_rows, CW).astype(BF16)).astype(BF16)
-    for c in range(NC):
-        xg[z, core, :, c * CW : (c + 1) * CW] = turned[c * ROWS : (c + 1) * ROWS, :]
+    turned = dot(turn, ib[...].astype(F32).reshape(own_rows, CA).astype(BF16)).astype(BF16)
+    for c in range(NC):
+        xa[z, core, :, c * CA : (c + 1) * CA] = turned[c * ROWS : (c + 1) * ROWS, :]
 
     def copy4(zz, h, dev):
-        block = xg.at[zz, core, pl.ds(h * HALF, HALF), :]
-        return pltpu.make_async_remote_copy(
-            src_ref=block, dst_ref=block, send_sem=s4, recv_sem=r4.at[zz * 2 + h], device_id=dev, device_id_type=MESH
-        )
+        block = xa.at[zz, core, pl.ds(h * HALF, HALF), :]
+        return remote(block, block, s4, r4.at[zz * 2 + h], dev)
 
     def cross4(zz, h, side):
-        block = xg.at[zz, side, pl.ds(h * HALF, HALF), :]
-        return pltpu.make_async_remote_copy(
-            src_ref=block, dst_ref=block, send_sem=s4d, recv_sem=r4d.at[zz * 2 + h], device_id=mate, device_id_type=MESH
-        )
+        block = xa.at[zz, side, pl.ds(h * HALF, HALF), :]
+        return remote(block, block, s4d, r4d.at[zz * 2 + h], mate)
 
     right, left = at_z(along(1)), at_z(along(-1))
     for h in range(2):
@@ -287,17 +344,33 @@
     cross4(z, 0, core).start()
     cross4(z, 1, core).start()
 
-    def run_expert(zz):
+    all_of(sg.at[pl.ds(0, NZ - 1)], rb1)
+    group = sg[...].reshape(qn, CB + TAIL)
+    for c in range(NC):
+        chosen_c = jnp.where(c_of_q == c, big_chosen, 0.0).astype(BF16)
+        picked = lax.dot_general(
+            chosen_c, group[:, :CB], (((0,), (0,)), ((), ())), preferred_element_type=F32
+        )
+        tb[:, :, c * CB : (c + 1) * CB] = picked.reshape(NE, NZ * SLOTS, CB).astype(BF16)
+    for dy, dx in ways:
+        e = over(dy, dx)
+        remote(tb.at[e], xr.at[core, ep], sb2, rb2.at[ep], (e, tp)).start()
+    xr[core, ep] = tb[ep]
+    remote(tb.at[ep], xr.at[core, ep], sb2d, rb2d, mate).start()
+
+    def across(first, last):
+        for dy, dx in ways[first:last]:
+            source = over(-dy, -dx)
+            block = xr.at[core, source]
+            remote(block, block, sb2, rb2.at[source], mate).wait_recv()
+            remote(block, block, sb2d, rb2d, mate).start()
+
+    all_of(wgu_a, lsem.at[8])
+
+    def first_part(zz):
         for h in range(2):
             cross4(zz, h, other).wait_recv()
-        rows = xg[zz].reshape(2 * ROWS, D)
-        gu = dot(rows, wgu[...])
-        gate, up = jnp.minimum(gu[:, :FW], CLAMP), jnp.clip(gu[:, FW:], -CLAMP, CLAMP)
-        act = ((up + 1.0) * (gate * jax.nn.sigmoid(ALPHA * gate))).astype(BF16)
-        part[zz] = dot(act, wdown[...]).astype(BF16).reshape(2, ROWS, D)
-        pltpu.make_async_remote_copy(
-            src_ref=part.at[zz, other], dst_ref=rpart.at[zz], send_sem=s5p, recv_sem=r5p.at[zz], device_id=mate, device_id_type=MESH
-        ).start()
+        acc[zz] = dot(xa[zz].reshape(2 * ROWS, DA), wgu_a[...])
 
     for s in range(1, 5):
         for i in range(2):
@@ -309,26 +382,52 @@
                         copy4(zz, h, nxt).start()
                     cross4(zz, h, core).start()
         if s == 1:
-            run_expert(z)
+            first_part(z)
         else:
-            pl.loop(0, 2)(lambda i, s=s: run_expert(along((s - 1) * (1 - 2 * i))))
+            pl.loop(0, 2)(lambda i, s=s: first_part(along((s - 1) * (1 - 2 * i))))
+    across(0, len(ways))
+    first_part(along(4))
+
+    tr, tc = iota((rn, rn), 0), iota((rn, rn), 1)
+    by_z = onehot(tc == ((tr // SLOTS) % NE) * 16 + (tr // ROWS) * SLOTS + tr % SLOTS).astype(BF16)
+    all_of(wgu_b, lsem.at[9])
+    all_of(wdown_a, lsem.at[10])
+    all_of(wdown_b, lsem.at[21])
+    xb[:, core] = dot(by_z, xr[core].reshape(rn, DB)).astype(BF16).reshape(NZ, ROWS, DB)
+    all_of(xr.at[core], rb2d)
+    xb[:, other] = dot(by_z, xr[other].reshape(rn, DB)).astype(BF16).reshape(NZ, ROWS, DB)
+
+    def pair_a(zz):
+        return remote(part_a.at[zz, other], rpart_a.at[zz], s5p, r5p.at[zz], mate)
+
+    def finish(one, two):
+        rows = jnp.concatenate([xb[one].reshape(2 * ROWS, DB), xb[two].reshape(2 * ROWS, DB)], axis=0)
+        gu = jnp.concatenate([acc[one], acc[two]], axis=0) + dot(rows, wgu_b[...])
+        gate, up = jnp.minimum(gu[:, :FW], CLAMP), jnp.clip(gu[:, FW:], -CLAMP, CLAMP)
+        act = ((up + 1.0) * (gate * jax.nn.sigmoid(ALPHA * gate))).astype(BF16)
+        out = dot(act, wdown_a[...]).astype(BF16)
+        part_a[one] = out[: 2 * ROWS].reshape(2, ROWS, DA)
+        part_a[two] = out[2 * ROWS :].reshape(2, ROWS, DA)
+        out = dot(act, wdown_b[...]).astype(BF16)
+        for i, zz in enumerate((one, two)):
+            for side in range(2):
+                at = (2 * i + side) * ROWS
+                part_b[side, zz] = out[at : at + ROWS]
+        for zz in (one, two):
+            pair_a(zz).start()
+            remote(part_b.at[other, zz], rpart_b.at[zz], sbp, rbp, mate).start()
+
     def pair_sum(zz, h):
         rows = slice(h * HALF, (h + 1) * HALF)
-        return part[zz, core, rows, :].astype(F32) + rpart[zz, rows, :].astype(F32)
-
-    def wait_pair(zz):
-        pltpu.make_async_remote_copy(
-            src_ref=part.at[zz, other], dst_ref=rpart.at[zz], send_sem=s5p, recv_sem=r5p.at[zz], device_id=mate, device_id_type=MESH
-        ).wait_recv()
+        return part_a[zz, core, rows, :].astype(F32) + rpart_a[zz, rows, :].astype(F32)
 
     def copy5(zz, h, hop, to_right):
-        return pltpu.make_async_remote_copy(
-            src_ref=sums.at[zz, h],
-            dst_ref=(rright if to_right else rleft).at[h, hop],
-            send_sem=s5,
-            recv_sem=(r5r if to_right else r5l).at[h * 4 + hop],
-            device_id=right if to_right else left,
-            device_id_type=MESH,
+        return remote(
+            sums.at[zz, h],
+            (rright if to_right else rleft).at[h, hop],
+            s5,
+            (r5r if to_right else r5l).at[h * 4 + hop],
+            right if to_right else left,
         )
 
     def got5(h, hop, from_left):
@@ -343,27 +442,39 @@
         sums[zz, h] = total.astype(BF16)
         copy5(zz, h, hop - 1, to_right).start()
 
-    wait_pair(along(3))
+    finish(along(3), along(-3))
+    finish(along(4), z)
+    pair_a(along(3)).wait_recv()
     pass_on(3, 1, True)
-    wait_pair(along(-3))
+    pair_a(along(-3)).wait_recv()
     pass_on(3, 0, False)
-    run_expert(along(4))
-    wait_pair(along(2))
-    wait_pair(along(-2))
-    wait_pair(along(4))
+    finish(along(2), along(-2))
+    pair_a(along(4)).wait_recv()
     pass_on(4, 0, True)
     pass_on(4, 1, False)
+    finish(along(1), along(-1))
+    pair_a(along(2)).wait_recv()
+    pair_a(along(-2)).wait_recv()
+
+    by_a = onehot(tr == ((tc // SLOTS) % NE) * 16 + (tc // ROWS) * SLOTS + tc % SLOTS).astype(BF16)
+    half_sum = dot(by_a, part_b[core].reshape(rn, DB))
+    all_of(rpart_b, rbp)
+    half_sum = half_sum + dot(by_a, rpart_b[...].reshape(rn, DB))
+    tb2[...] = half_sum.astype(BF16).reshape(NE, NZ * SLOTS, DB)
+    to_experts(tb2, rr, sb3, rb3)
+    rr[ep] = tb2[ep]
+
     for hop in (2, 1):
         pass_on(hop, 1, True)
         pass_on(hop, 0, False)
         if hop == 2:
-            wait_pair(along(1))
-            wait_pair(along(-1))
+            pair_a(along(1)).wait_recv()
+            pair_a(along(-1)).wait_recv()
         pass_on(hop + 1, 0, True)
         pass_on(hop + 1, 1, False)
     pass_on(1, 0, True)
     pass_on(1, 1, False)
-    wait_pair(z)
+    pair_a(z).wait_recv()
     for h in range(2):
         total = pair_sum(z, h)
         for to_right in (True, False):
@@ -371,35 +482,64 @@
             total = total + got5(h, 0, to_right)
         sums[z, h] = total.astype(BF16)
 
-    mine = jnp.concatenate([sums[z].reshape(ROWS, D)[:, c * CW : (c + 1) * CW] for c in range(NC)], axis=0)
+    mine = jnp.concatenate([sums[z].reshape(ROWS, DA)[:, c * CA : (c + 1) * CA] for c in range(NC)], axis=0)
     back = onehot(sr == ((sc // SLOTS) % NE) * 8 + (sc // ROWS) * SLOTS + sc % SLOTS).astype(BF16)
-    ob2[...] = dot(back, mine).reshape(NE, 8, CW).astype(BF16)
+    ob2[...] = dot(back, mine).reshape(NE, 8, CA).astype(BF16)
     ib2[ep] = ob2[ep]
-    for d in far:
-        copy3((ep + d) % NE, ob2, ib2, s6, r6).start()
+    to_experts(ob2, ib2, s6, r6)
+
+    def in_two(values):
+        high = values.astype(BF16)
+        return high, (values - high.astype(F32)).astype(BF16)
+
+    tails = sg[...].reshape(qn, CB + TAIL)[:, CB:].astype(F32)
+    big_weighed = jnp.zeros(big_q, F32)
+    for k in range(4):
+        weight = tails[:, k : k + 1] + tails[:, 4 + k : 5 + k]
+        big_weighed = big_weighed + onehot(core_ids[:, k : k + 1] == big_e) * weight
+    big_high, big_low = in_two(big_chosen * big_weighed)
+    all_of(rr.at[pl.ds(0, NE - 1)], rb3)
+    taken = rr[...].reshape(rn, DB)
+    mixed = jnp.zeros((qn, CB), F32)
+    for c in range(NC):
+        piece = taken[:, c * CB : (c + 1) * CB]
+        for factor in (big_low, big_high):
+            mixed = mixed + dot(jnp.where(c_of_q == c, factor.astype(F32), 0.0).astype(BF16), piece)
+    cb[...] = mixed.astype(BF16).reshape(NZ, 16, CB)
+    for d in (4, 3, 5, 2, 6, 1, 7):
+        remote(cb.at[along(d)], rcb.at[z], sb4, rb4, at_z(along(d))).start()
+    rcb[z] = cb[z]
+
     high = combine.astype(BF16)
     rest = combine - high.astype(F32)
-    middle = rest.astype(BF16)
-    lowest = (rest - middle.astype(F32)).astype(BF16)
-    pltpu.make_async_copy(ob2.at[pl.ds(0, NE - 1)], ib2.at[pl.ds(0, NE - 1)], r6).wait()
-    returned = ib2[...].astype(F32).reshape(NE * 8, CW).astype(BF16)
-    mix = dot(lowest, returned) + dot(middle, returned) + dot(high, returned)
-    tok_s[...] = tok_s[...] + mix
+    middle, lowest = in_two(rest)
+    all_of(ib2.at[pl.ds(0, NE - 1)], r6)
+    returned = ib2[...].astype(F32).reshape(NE * 8, CA).astype(BF16)
+    mix_a = dot(lowest, returned) + dot(middle, returned) + dot(high, returned)
+    all_of(rcb.at[pl.ds(0, NZ - 1)], rb4)
+    mix_b = jnp.zeros((16, CB), F32)
+    for zz in range(NZ):
+        mix_b = mix_b + rcb[zz].astype(F32)
+    tok_s[:, :CA] = tok_s[:, :CA] + mix_a
+    tok_s[:, CA:] = tok_s[:, CA:] + mix_b
     for c in range(NC):
         result_ref[:, c * CW : (c + 1) * CW] = tok_s[c * TOK : (c + 1) * TOK, :].astype(BF16)
 
-    def drain(ref, sem):
-        pltpu.make_async_copy(ref, ref, sem).wait()
-
-    drain(g1.at[pl.ds(0, NT - 1)], s1)
+    all_of(g1.at[pl.ds(0, NT - 1)], s1)
     pair2.wait_send()
-    drain(sb.at[pl.ds(0, NZ - 1)], s2)
-    drain(ob.at[pl.ds(0, NE - 1)], s3)
-    drain(xg.at[pl.ds(0, NZ - 1), 0], s4)
-    drain(xg.at[:, 0], s4d)
-    drain(rpart, s5p)
-    drain(sums.at[pl.ds(0, NZ - 1)], s5)
-    drain(ob2.at[pl.ds(0, NE - 1)], s6)
+    all_of(sb.at[pl.ds(0, NZ - 1)], s2)
+    all_of(ob.at[pl.ds(0, NE - 1)], s3)
+    all_of(xa.at[pl.ds(0, NZ - 1), 0], s4)
+    all_of(xa.at[:, 0], s4d)
+    all_of(rpart_a, s5p)
+    all_of(sums.at[pl.ds(0, NZ - 1)], s5)
+    all_of(ob2.at[pl.ds(0, NE - 1)], s6)
+    all_of(sg.at[pl.ds(0, NZ - 1)], sb1)
+    all_of(tb.at[pl.ds(0, NE - 1)], sb2)
+    all_of(tb, sb2d)
+    all_of(rpart_b, sbp)
+    all_of(tb2.at[pl.ds(0, NE - 1)], sb3)
+    all_of(cb.at[pl.ds(0, NZ - 1)], sb4)
 
 
 def per_device(
@@ -419,16 +559,20 @@
             v(tokens.shape, BF16), v((D // W, W), BF16), v((TOK, seqs), I32), v((TOK, TOK), F32),
             v((seqs, W), F32), v((3, seqs, W), BF16), v((NT, W), F32), v((NT, W), BF16), v((D // W, W), BF16), v((TOK, W), BF16),
             v((D, 2 * W), BF16), v((NC * W, CW), BF16), v((W, W), BF16), v((W, W), BF16),
-            v((D, 2 * FW), BF16), v((FW, D), BF16),
+            v((DA, 2 * FW), BF16), v((DB, 2 * FW), BF16), v((FW, DA), BF16), v((FW, DB), BF16),
             v((16, CW), F32), v((NT, 16, CW), BF16),
             v((2, NZ, 16, CW + TAIL), BF16), v((NZ, 16, CW + TAIL), BF16), v((NZ, 16, CW + TAIL), BF16),
             v((NZ, 16, CW + TAIL), BF16),
-            v((NE, 8, CW), BF16), v((NE, 8, CW), BF16),
-            v((NZ, 2, ROWS, D), BF16), v((NZ, 2, ROWS, D), BF16), v((NZ, ROWS, D), BF16),
-            v((NZ, 2, HALF, D), BF16), v((2, 4, HALF, D), BF16), v((2, 4, HALF, D), BF16),
-            v((NE, 8, CW), BF16), v((NE, 8, CW), BF16), v((16, 4), F32),
-            dma((21,)), dma, dma((NT,)), dma, dma, dma, dma, dma, dma,
+            v((NE, 8, CA), BF16), v((NE, 8, CA), BF16),
+            v((NZ, 2, ROWS, DA), BF16), v((NZ, 2 * ROWS, 2 * FW), F32), v((NZ, 2, ROWS, DA), BF16), v((NZ, ROWS, DA), BF16),
+            v((NZ, 2, HALF, DA), BF16), v((2, 4, HALF, DA), BF16), v((2, 4, HALF, DA), BF16),
+            v((NE, 8, CA), BF16), v((NE, 8, CA), BF16), v((16, 4), F32),
+            v((NZ, 16, CB + TAIL), BF16), v((NE, 16, DB), BF16), v((2, NE, 16, DB), BF16), v((NZ, 2, ROWS, DB), BF16),
+            v((2, NZ, ROWS, DB), BF16), v((NZ, ROWS, DB), BF16), v((NE, 16, DB), BF16), v((NE, 16, DB), BF16),
+            v((NZ, 16, CB), BF16), v((NZ, 16, CB), BF16),
+            dma((22,)), dma, dma((NT,)), dma, dma, dma, dma, dma, dma,
             dma, dma((NZ * 2,)), dma, dma((NZ * 2,)), dma, dma((NZ,)), dma, dma((8,)), dma((8,)), dma, dma,
+            dma, dma, dma, dma((NE,)), dma, dma, dma, dma, dma, dma, dma, dma,
         ],
         compiler_params=pltpu.CompilerParams(
             collective_id=0, has_side_effects=True, vmem_limit_bytes=60 * 1024 * 1024

time: 94.6 us -> 85.3 us (0.902)
  Pallas kernels: 92 us -> 82.6 us
    pallas_call x1, Pallas kernels: 92 us -> 82.6 us  [per_device(): pl.pallas_call(kernel, name='layer', out_shape=(v(tokens.shape, BF16), v(...]
where the time goes in v3:
time: 85.3 us; the launch traced here: 85.1 us
  Pallas kernels  82.6 us (97%)
  local copies, waits for them, and re-layouts  1.85 us (2%)
    pallas_call x1, Pallas kernels, per_device(): pl.pallas_call(kernel, name='layer', out_shape=(v(tokens.shape, BF16), v(...  82.6 us
    unnamed x3, local copies, waits for them, and re-layouts  1.85 us

profile of v3, /device:TPU:2, one launch (start us, length us, event | category | flops | bytes accessed | tf_op | source)
XLA Modules:
  0.0 85.1 jit_solution(16065732475944067812)
XLA Ops:
  0.6 82.6 %layer.1 = (bf16[4,4096]{1,0:T(4,128)(2,1)S(1)}, f32[64,128]{1,0:T(8,128)S(1)}, bf16[3,64,128]{2,1,0:T(8,128)(2,1)S(1)}) custom-call(bf16[4,4096]{1,0:T(4,128)(2,1)} %tokens_hbm.1, bf16[32,128]{1,0:T(8,128)(2,1)} %bitcast.9, s32[4,64]{1,0:T(4,128)} %bitcast.13, f32[4,4]{1,0:T(4,128)} %weights_hbm.1, f32[64,128]{1,0:T(8,128)} %rec_hbm.1, ...), custom_call_target="tpu_custom_call" | custom-call | tf_op jit(solution)/shard_map/layer/pallas_call | solution.py:552
  83.2 0.6 copy.24
  83.8 0.6 copy.25
  84.4 0.6 copy.26

commit v4 on v3

--- a/solution.py
+++ b/solution.py
@@ -26,10 +26,12 @@
 SLOTS = 2
 ROWS = NE * SLOTS
 HALF = ROWS // 2
+QUARTER = ROWS // 4
 TAIL = 128
-CB = 384
-CA = CW - CB
-DA, DB = NC * CA, NC * CB
+EARLY = 5
+CBI, CBO = 512, 384
+CAI, CAO = CW - CBI, CW - CBO
+DAI, DBI, DAO, DBO = NC * CAI, NC * CBI, NC * CAO, NC * CBO
 
 
 def iota(shape, dim):
@@ -77,8 +79,9 @@
     pin_hbm, pgate_hbm, bdec_hbm, binp_hbm, pout_hbm, eg_hbm, eu_hbm, ed_hbm,
     result_ref, state_ref, newconv_ref,
     tokens_ref, gain1_ref, ids_ref, weights_ref, rec_ref, conv_ref, logit_ref, rgain_ref, gain2_ref, taps_ref,
-    wcat, w4, bdec, binp, wgu_a, wgu_b, wdown_a, wdown_b,
+    wcat, w4, gates, wgu_a, wgu_b, wdown_a, wdown_b,
     tok_s, g1, pb, rp, sb, rb, ob, ib, xa, acc, part_a, rpart_a, sums, rright, rleft, ob2, ib2, rw_s,
+    perm_s, expand_s, by_z_s, by_a_s, chosen_s,
     sg, tb, xr, xb, part_b, rpart_b, tb2, rr, cb, rcb,
     lsem, s1, r1, s2p, r2p, s2, r2, s3, r3, s4, r4, s4d, r4d, s5p, r5p, s5, r5r, r5l, s6, r6,
     sb1, rb1, sb2, rb2, sb2d, rb2d, sbp, rbp, sb3, rb3, sb4, rb4,
@@ -96,6 +99,9 @@
             src_ref=src, dst_ref=dst, send_sem=ss, recv_sem=rs, device_id=dev, device_id_type=MESH
         )
 
+    def all_of(ref, sem):
+        pltpu.make_async_copy(ref, ref, sem).wait()
+
     def over(dy, dx):
         return ((y + dy + 4) % 4) * 4 + (x + dx + 4) % 4
 
@@ -113,7 +119,7 @@
         pl.semaphore_signal(barrier, inc=1, device_id=((ep + d) % NE, tp), device_id_type=MESH)
 
     smalls = [
-        pltpu.make_async_copy(src, dst, lsem.at[11 + i])
+        pltpu.make_async_copy(src, dst, lsem.at[7 + i])
         for i, (src, dst) in enumerate((
             (tokens_hbm, tokens_ref), (gain1_hbm, gain1_ref), (ids_hbm, ids_ref), (weights_hbm, weights_ref),
             (rec_hbm, rec_ref), (conv_hbm, conv_ref), (logit_hbm, logit_ref), (rgain_hbm, rgain_ref),
@@ -124,27 +130,27 @@
         load.start()
     loads = [
         pltpu.make_async_copy(pin_hbm, wcat.at[:, pl.ds(0, W)], lsem.at[0]),
-        pltpu.make_async_copy(pgate_hbm, wcat.at[:, pl.ds(W, W)], lsem.at[1]),
-        pltpu.make_async_copy(bdec_hbm.at[tp], bdec, lsem.at[2]),
-        pltpu.make_async_copy(binp_hbm.at[tp], binp, lsem.at[3]),
+        pltpu.make_async_copy(pgate_hbm, wcat.at[:, pl.ds(W, W)], lsem.at[0]),
+        pltpu.make_async_copy(bdec_hbm.at[tp], gates.at[0], lsem.at[1]),
+        pltpu.make_async_copy(binp_hbm.at[tp], gates.at[1], lsem.at[1]),
     ]
     for c in range(NC):
         loads.append(
             pltpu.make_async_copy(
-                pout_hbm.at[:, pl.ds(c * CW, CW)], w4.at[pl.ds(c * W, W), :], lsem.at[4 + c]
+                pout_hbm.at[:, pl.ds(c * CW, CW)], w4.at[pl.ds(c * W, W), :], lsem.at[2]
             )
         )
     for load in loads:
         load.start()
     for c in range(NC):
         for i, (hbm, col) in enumerate(((eg_hbm, 0), (eu_hbm, FW))):
-            for dst, first, size, sem in ((wgu_a, 0, CA, 8), (wgu_b, CA, CB, 9)):
+            for dst, first, size, sem in ((wgu_a, 0, CAI, 3), (wgu_b, CAI, CBI, 4)):
                 pltpu.make_async_copy(
                     hbm.at[0, pl.ds(c * CW + first, size), :],
                     dst.at[pl.ds(c * size, size), pl.ds(col, FW)],
                     lsem.at[sem],
                 ).start()
-        for dst, first, size, sem in ((wdown_a, 0, CA, 10), (wdown_b, CA, CB, 21)):
+        for dst, first, size, sem in ((wdown_a, 0, CAO, 5), (wdown_b, CAO, CBO, 6)):
             pltpu.make_async_copy(
                 ed_hbm.at[0, :, pl.ds(c * CW + first, size)], dst.at[:, pl.ds(c * size, size)], lsem.at[sem]
             ).start()
@@ -160,14 +166,9 @@
 
     pl.semaphore_wait(barrier, NZ + NE - 1)
 
-    def copy1(dev, slot):
-        return pltpu.make_async_remote_copy(
-            src_ref=g1.at[slot], dst_ref=g1.at[slot], send_sem=s1, recv_sem=r1.at[slot], device_id=dev, device_id_type=MESH
-        )
-
     for d in (4, 3, 5, 2, 6, 1, 7):
-        copy1(at_z(along(d)), tp).start()
-    copy1(mate, tp).start()
+        remote(g1.at[tp], g1.at[tp], s1, r1.at[z], at_z(along(d))).start()
+    remote(g1.at[tp], g1.at[tp], s1, r1.at[NZ], mate).start()
 
     q4, r4e = (NC * TOK, W), 8
     row_n, row_c = iota(q4, 0) % TOK, iota(q4, 0) // TOK
@@ -213,20 +214,30 @@
     big_before = dot(big_earlier.astype(BF16), big_hit.astype(BF16))
     big_chosen = big_hit * onehot((big_before == big_s) & same_z)
     c_of_q = (iota(big_q, 0) // TOK) % NC
-
-    for d in (1, 7, 2, 6, 3, 5, 4):
-        slot = along(d) * 2 + core
-        copy1(mate, slot).wait_recv()
-        copy1(mate, slot).start()
-    for d in range(NZ):
-        copy1(mate, along(d) * 2 + other).wait_recv()
+    for c in range(NC):
+        chosen_s[c] = jnp.where(c_of_q == c, big_chosen, 0.0).astype(BF16)
 
     big = NT * NC * TOK
     pr, pc = iota((big, big), 0), iota((big, big), 1)
-    perm = onehot(pc == ((pr // TOK) % NT) * 16 + (pr // 64) * TOK + pr % TOK).astype(BF16)
-    stacked = dot(perm, g1[...].reshape(big, CW)).astype(BF16)
-    for load in loads[0:4] + smalls[4:]:
+    perm_s[...] = onehot(pc == ((pr // TOK) % NT) * 16 + (pr // 64) * TOK + pr % TOK).astype(BF16)
+    er, et = iota((big, NT * TOK), 0), iota((big, NT * TOK), 1)
+    expand_s[...] = onehot(et == (((er // 16) % NZ) * 2 + er // 128) * TOK + er % TOK).astype(BF16)
+    tr, tc = iota((rn, rn), 0), iota((rn, rn), 1)
+    by_z_s[...] = onehot(tc == ((tr // SLOTS) % NE) * 16 + (tr // ROWS) * SLOTS + tr % SLOTS).astype(BF16)
+    by_a_s[...] = onehot(tr == ((tc // SLOTS) % NE) * 16 + (tc // ROWS) * SLOTS + tc % SLOTS).astype(BF16)
+
+    for d in (1, 7, 2, 6, 3, 5, 4):
+        zz = along(d)
+        block = g1.at[zz * 2 + core]
+        remote(block, block, s1, r1.at[zz], mate).wait_recv()
+        remote(block, block, s1, r1.at[NZ], mate).start()
+    all_of(g1.at[pl.ds(0, NZ)], r1.at[NZ])
+
+    stacked = dot(perm_s[...], g1[...].reshape(big, CW)).astype(BF16)
+    for load in smalls[4:]:
         load.wait()
+    all_of(wcat, lsem.at[0])
+    all_of(gates, lsem.at[1])
     both = jnp.zeros((NT * TOK, 2 * W), F32)
     for c in range(NC):
         both = both + dot(stacked[c * 64 : (c + 1) * 64, :], wcat[c * CW : (c + 1) * CW, :])
@@ -241,8 +252,8 @@
     newconv_ref[2] = joined[:, :W]
 
     low = conv.astype(BF16)
-    decay_gate = jax.nn.sigmoid(dot(low, bdec[...]))
-    input_gate = jax.nn.sigmoid(dot(low, binp[...]))
+    decay_gate = jax.nn.sigmoid(dot(low, gates[0]))
+    input_gate = jax.nn.sigmoid(dot(low, gates[1]))
     mine = iota((NT, W), 0) == tp
     logit = jnp.sum(jnp.where(mine, logit_ref[...], 0.0), axis=0, keepdims=True)
     rgain = jnp.sum(jnp.where(mine, rgain_ref[...].astype(F32), 0.0), axis=0, keepdims=True)
@@ -253,13 +264,10 @@
     hidden = new_state * jax.nn.gelu(branch_gate)
     squares = jnp.broadcast_to(jnp.sum(hidden * hidden, axis=1, keepdims=True), (NT * TOK, W))
 
-    er, et = iota((big, NT * TOK), 0), iota((big, NT * TOK), 1)
-    expand = onehot(et == (((er // 16) % NZ) * 2 + er // 128) * TOK + er % TOK).astype(BF16)
-    wide = dot(expand, jnp.concatenate([(hidden * rgain).astype(BF16), squares.astype(BF16)], axis=1))
+    wide = dot(expand_s[...], jnp.concatenate([(hidden * rgain).astype(BF16), squares.astype(BF16)], axis=1))
     gained, sq_wide = wide[:, :W], wide[:, W:]
     c_of = (iota((big, W), 0) // TOK) % NC
-    for load in loads[4:8]:
-        load.wait()
+    all_of(w4, lsem.at[2])
     lhs = jnp.concatenate([jnp.where(c_of == c, gained, 0.0) for c in range(NC)], axis=1).astype(BF16)
     pb[:, :, :, 0:CW] = dot(lhs, w4[...]).astype(BF16).reshape(2, NZ, 16, CW)
     pb[:, :, :, CW : CW + TAIL] = sq_wide.astype(BF16).reshape(2, NZ, 16, TAIL)
@@ -296,12 +304,12 @@
     for k in range(4):
         tail = jnp.where(lane == k, w_high[:, k : k + 1], tail)
         tail = jnp.where(lane == 4 + k, w_rest[:, k : k + 1], tail)
-    sg[z, :, 0:CB] = second[:, CA:]
-    sg[z, :, CB:] = tail.astype(BF16)
+    sg[z, :, 0:CBI] = second[:, CAI:]
+    sg[z, :, CBI:] = tail.astype(BF16)
     sent = lax.dot_general(
-        chosen.astype(BF16), second[:, :CA], (((0,), (0,)), ((), ())), preferred_element_type=F32
-    )
-    ob[...] = sent.reshape(NE, 8, CA).astype(BF16)
+        chosen.astype(BF16), second[:, :CAI], (((0,), (0,)), ((), ())), preferred_element_type=F32
+    )
+    ob[...] = sent.reshape(NE, 8, CAI).astype(BF16)
     ib[ep] = ob[ep]
     for d in (4, 3, 5, 2, 6, 1, 7):
         remote(sg.at[z], sg.at[z], sb1, rb1, at_z(along(d))).start()
@@ -318,16 +326,13 @@
 
     to_experts(ob, ib, s3, r3)
 
-    def all_of(ref, sem):
-        pltpu.make_async_copy(ref, ref, sem).wait()
-
     all_of(ib.at[pl.ds(0, NE - 1)], r3)
     own_rows = NE * 8
     sr, sc = iota((own_rows, own_rows), 0), iota((own_rows, own_rows), 1)
     turn = onehot(sc == ((sr // SLOTS) % NE) * 8 + (sr // ROWS) * SLOTS + sr % SLOTS).astype(BF16)
-    turned = dot(turn, ib[...].astype(F32).reshape(own_rows, CA).astype(BF16)).astype(BF16)
-    for c in range(NC):
-        xa[z, core, :, c * CA : (c + 1) * CA] = turned[c * ROWS : (c + 1) * ROWS, :]
+    turned = dot(turn, ib[...].astype(F32).reshape(own_rows, CAI).astype(BF16)).astype(BF16)
+    for c in range(NC):
+        xa[z, core, :, c * CAI : (c + 1) * CAI] = turned[c * ROWS : (c + 1) * ROWS, :]
 
     def copy4(zz, h, dev):
         block = xa.at[zz, core, pl.ds(h * HALF, HALF), :]
@@ -335,7 +340,7 @@
 
     def cross4(zz, h, side):
         block = xa.at[zz, side, pl.ds(h * HALF, HALF), :]
-        return remote(block, block, s4d, r4d.at[zz * 2 + h], mate)
+        return remote(block, block, s4d, r4d.at[zz], mate)
 
     right, left = at_z(along(1)), at_z(along(-1))
     for h in range(2):
@@ -345,34 +350,36 @@
     cross4(z, 1, core).start()
 
     all_of(sg.at[pl.ds(0, NZ - 1)], rb1)
-    group = sg[...].reshape(qn, CB + TAIL)
-    for c in range(NC):
-        chosen_c = jnp.where(c_of_q == c, big_chosen, 0.0).astype(BF16)
+    group = sg[...].reshape(qn, CBI + TAIL)
+    for c in range(NC):
         picked = lax.dot_general(
-            chosen_c, group[:, :CB], (((0,), (0,)), ((), ())), preferred_element_type=F32
+            chosen_s[c], group[:, :CBI], (((0,), (0,)), ((), ())), preferred_element_type=F32
         )
-        tb[:, :, c * CB : (c + 1) * CB] = picked.reshape(NE, NZ * SLOTS, CB).astype(BF16)
-    for dy, dx in ways:
+        tb[:, :, c * CBI : (c + 1) * CBI] = picked.reshape(NE, NZ * SLOTS, CBI).astype(BF16)
+    for i, (dy, dx) in enumerate(ways):
         e = over(dy, dx)
-        remote(tb.at[e], xr.at[core, ep], sb2, rb2.at[ep], (e, tp)).start()
+        remote(tb.at[e], xr.at[core, ep], sb2, rb2.at[min(i // EARLY, 2)], (e, tp)).start()
     xr[core, ep] = tb[ep]
     remote(tb.at[ep], xr.at[core, ep], sb2d, rb2d, mate).start()
 
-    def across(first, last):
+    def across(first, last, group):
+        all_of(tb.at[pl.ds(0, last - first)], rb2.at[group])
         for dy, dx in ways[first:last]:
             source = over(-dy, -dx)
             block = xr.at[core, source]
-            remote(block, block, sb2, rb2.at[source], mate).wait_recv()
             remote(block, block, sb2d, rb2d, mate).start()
 
-    all_of(wgu_a, lsem.at[8])
-
-    def first_part(zz):
-        for h in range(2):
-            cross4(zz, h, other).wait_recv()
-        acc[zz] = dot(xa[zz].reshape(2 * ROWS, DA), wgu_a[...])
-
-    for s in range(1, 5):
+    all_of(wgu_a, lsem.at[3])
+
+    def first_part(*blocks):
+        for zz in blocks:
+            all_of(xa.at[zz, other], r4d.at[zz])
+        rows = jnp.concatenate([xa[zz].reshape(2 * ROWS, DAI) for zz in blocks], axis=0)
+        out = dot(rows, wgu_a[...])
+        for i, zz in enumerate(blocks):
+            acc[zz] = out[i * 2 * ROWS : (i + 1) * 2 * ROWS].reshape(2, ROWS, 2 * FW)
+
+    def arrivals(s):
         for i in range(2):
             for h, way, hops, nxt in ((i, -1, 4 - i, right), (1 - i, 1, 4 - i, left)):
                 if s <= hops:
@@ -381,44 +388,49 @@
                     if s < hops:
                         copy4(zz, h, nxt).start()
                     cross4(zz, h, core).start()
-        if s == 1:
-            first_part(z)
-        else:
-            pl.loop(0, 2)(lambda i, s=s: first_part(along((s - 1) * (1 - 2 * i))))
-    across(0, len(ways))
-    first_part(along(4))
-
-    tr, tc = iota((rn, rn), 0), iota((rn, rn), 1)
-    by_z = onehot(tc == ((tr // SLOTS) % NE) * 16 + (tr // ROWS) * SLOTS + tr % SLOTS).astype(BF16)
-    all_of(wgu_b, lsem.at[9])
-    all_of(wdown_a, lsem.at[10])
-    all_of(wdown_b, lsem.at[21])
-    xb[:, core] = dot(by_z, xr[core].reshape(rn, DB)).astype(BF16).reshape(NZ, ROWS, DB)
+
+    def turn_over(side):
+        xb[:, side] = dot(by_z_s[...], xr[side].reshape(rn, DBI)).astype(BF16).reshape(NZ, ROWS, DBI)
+
+    arrivals(1)
+    first_part(z)
+    arrivals(2)
+    first_part(along(1), along(-1))
+    across(0, EARLY, 0)
+    arrivals(3)
+    across(EARLY, 2 * EARLY, 1)
+    first_part(along(2), along(-2))
+    across(2 * EARLY, len(ways), 2)
+    arrivals(4)
+    turn_over(core)
+    all_of(wgu_b, lsem.at[4])
+    all_of(wdown_a, lsem.at[5])
+    all_of(wdown_b, lsem.at[6])
+    first_part(along(3), along(-3), along(4))
     all_of(xr.at[core], rb2d)
-    xb[:, other] = dot(by_z, xr[other].reshape(rn, DB)).astype(BF16).reshape(NZ, ROWS, DB)
+    turn_over(other)
 
     def pair_a(zz):
         return remote(part_a.at[zz, other], rpart_a.at[zz], s5p, r5p.at[zz], mate)
 
-    def finish(one, two):
-        rows = jnp.concatenate([xb[one].reshape(2 * ROWS, DB), xb[two].reshape(2 * ROWS, DB)], axis=0)
-        gu = jnp.concatenate([acc[one], acc[two]], axis=0) + dot(rows, wgu_b[...])
+    def finish(*blocks):
+        rows = jnp.concatenate([xb[zz].reshape(2 * ROWS, DBI) for zz in blocks], axis=0)
+        gu = jnp.concatenate([acc[zz].reshape(2 * ROWS, 2 * FW) for zz in blocks], axis=0) + dot(rows, wgu_b[...])
         gate, up = jnp.minimum(gu[:, :FW], CLAMP), jnp.clip(gu[:, FW:], -CLAMP, CLAMP)
         act = ((up + 1.0) * (gate * jax.nn.sigmoid(ALPHA * gate))).astype(BF16)
         out = dot(act, wdown_a[...]).astype(BF16)
-        part_a[one] = out[: 2 * ROWS].reshape(2, ROWS, DA)
-        part_a[two] = out[2 * ROWS :].reshape(2, ROWS, DA)
+        for i, zz in enumerate(blocks):
+            part_a[zz] = out[2 * i * ROWS : 2 * (i + 1) * ROWS].reshape(2, ROWS, DAO)
+            pair_a(zz).start()
         out = dot(act, wdown_b[...]).astype(BF16)
-        for i, zz in enumerate((one, two)):
+        for i, zz in enumerate(blocks):
             for side in range(2):
                 at = (2 * i + side) * ROWS
                 part_b[side, zz] = out[at : at + ROWS]
-        for zz in (one, two):
-            pair_a(zz).start()
             remote(part_b.at[other, zz], rpart_b.at[zz], sbp, rbp, mate).start()
 
     def pair_sum(zz, h):
-        rows = slice(h * HALF, (h + 1) * HALF)
+        rows = slice(h * QUARTER, (h + 1) * QUARTER)
         return part_a[zz, core, rows, :].astype(F32) + rpart_a[zz, rows, :].astype(F32)
 
     def copy5(zz, h, hop, to_right):
@@ -436,55 +448,85 @@
     def pass_on(hop, h, to_right):
         zz = along(hop if to_right else -hop)
         total = pair_sum(zz, h)
-        if hop < (4 - h if to_right else 3 + h):
+        if hop < (4 - h // 2 if to_right else 3 + h // 2):
             copy5(zz, h, hop, to_right).wait_recv()
             total = total + got5(h, hop, to_right)
         sums[zz, h] = total.astype(BF16)
         copy5(zz, h, hop - 1, to_right).start()
 
+    def pair_sum(zz, h):
+        rows = slice(h * QUARTER, (h + 1) * QUARTER)
+        return part_a[zz, core, rows, :].astype(F32) + rpart_a[zz, rows, :].astype(F32)
+
+    def copy5(zz, h, hop, to_right):
+        return remote(
+            sums.at[zz, h],
+            (rright if to_right else rleft).at[h, hop],
+            s5,
+            (r5r if to_right else r5l).at[h * 4 + hop],
+            right if to_right else left,
+        )
+
+    def got5(h, hop, from_left):
+        return (rright if from_left else rleft)[h, hop].astype(F32)
+
+    def pass_on(hop, h, to_right):
+        zz = along(hop if to_right else -hop)
+        total = pair_sum(zz, h)
+        if hop < (4 - h // 2 if to_right else 3 + h // 2):
+            copy5(zz, h, hop, to_right).wait_recv()
+            total = total + got5(h, hop, to_right)
+        sums[zz, h] = total.astype(BF16)
+        copy5(zz, h, hop - 1, to_right).start()
+
+    def shorter(hop):
+        for h in (0, 1):
+            pass_on(hop, h + 2, True)
+            pass_on(hop, h, False)
+
+    def longer(hop):
+        for h in (0, 1):
+            pass_on(hop, h, True)
+            pass_on(hop, h + 2, False)
+
     finish(along(3), along(-3))
     finish(along(4), z)
     pair_a(along(3)).wait_recv()
-    pass_on(3, 1, True)
     pair_a(along(-3)).wait_recv()
-    pass_on(3, 0, False)
+    shorter(3)
     finish(along(2), along(-2))
     pair_a(along(4)).wait_recv()
-    pass_on(4, 0, True)
-    pass_on(4, 1, False)
+    longer(4)
     finish(along(1), along(-1))
     pair_a(along(2)).wait_recv()
     pair_a(along(-2)).wait_recv()
-
-    by_a = onehot(tr == ((tc // SLOTS) % NE) * 16 + (tc // ROWS) * SLOTS + tc % SLOTS).astype(BF16)
-    half_sum = dot(by_a, part_b[core].reshape(rn, DB))
+    shorter(2)
+
+    half_sum = dot(by_a_s[...], part_b[core].reshape(rn, DBO))
     all_of(rpart_b, rbp)
-    half_sum = half_sum + dot(by_a, rpart_b[...].reshape(rn, DB))
-    tb2[...] = half_sum.astype(BF16).reshape(NE, NZ * SLOTS, DB)
+    half_sum = half_sum + dot(by_a_s[...], rpart_b[...].reshape(rn, DBO))
+    tb2[...] = half_sum.astype(BF16).reshape(NE, NZ * SLOTS, DBO)
     to_experts(tb2, rr, sb3, rb3)
     rr[ep] = tb2[ep]
 
-    for hop in (2, 1):
-        pass_on(hop, 1, True)
-        pass_on(hop, 0, False)
-        if hop == 2:
-            pair_a(along(1)).wait_recv()
-            pair_a(along(-1)).wait_recv()
-        pass_on(hop + 1, 0, True)
-        pass_on(hop + 1, 1, False)
-    pass_on(1, 0, True)
-    pass_on(1, 1, False)
+    longer(3)
+    pair_a(along(1)).wait_recv()
+    pair_a(along(-1)).wait_recv()
+    shorter(1)
+    longer(2)
+    longer(1)
     pair_a(z).wait_recv()
-    for h in range(2):
+    for h in (2, 3, 0, 1):
         total = pair_sum(z, h)
         for to_right in (True, False):
             copy5(z, h, 0, to_right).wait_recv()
             total = total + got5(h, 0, to_right)
         sums[z, h] = total.astype(BF16)
 
-    mine = jnp.concatenate([sums[z].reshape(ROWS, DA)[:, c * CA : (c + 1) * CA] for c in range(NC)], axis=0)
+    final = sums[z].astype(F32).reshape(ROWS, DAO).astype(BF16)
+    mine = jnp.concatenate([final[:, c * CAO : (c + 1) * CAO] for c in range(NC)], axis=0)
     back = onehot(sr == ((sc // SLOTS) % NE) * 8 + (sc // ROWS) * SLOTS + sc % SLOTS).astype(BF16)
-    ob2[...] = dot(back, mine).reshape(NE, 8, CA).astype(BF16)
+    ob2[...] = dot(back, mine).reshape(NE, 8, CAO).astype(BF16)
     ib2[ep] = ob2[ep]
     to_experts(ob2, ib2, s6, r6)
 
@@ -492,20 +534,20 @@
         high = values.astype(BF16)
         return high, (values - high.astype(F32)).astype(BF16)
 
-    tails = sg[...].reshape(qn, CB + TAIL)[:, CB:].astype(F32)
+    tails = sg[...].reshape(qn, CBI + TAIL)[:, CBI:].astype(F32)
     big_weighed = jnp.zeros(big_q, F32)
     for k in range(4):
         weight = tails[:, k : k + 1] + tails[:, 4 + k : 5 + k]
         big_weighed = big_weighed + onehot(core_ids[:, k : k + 1] == big_e) * weight
     big_high, big_low = in_two(big_chosen * big_weighed)
     all_of(rr.at[pl.ds(0, NE - 1)], rb3)
-    taken = rr[...].reshape(rn, DB)
-    mixed = jnp.zeros((qn, CB), F32)
-    for c in range(NC):
-        piece = taken[:, c * CB : (c + 1) * CB]
+    taken = rr[...].reshape(rn, DBO)
+    mixed = jnp.zeros((qn, CBO), F32)
+    for c in range(NC):
+        piece = taken[:, c * CBO : (c + 1) * CBO]
         for factor in (big_low, big_high):
             mixed = mixed + dot(jnp.where(c_of_q == c, factor.astype(F32), 0.0).astype(BF16), piece)
-    cb[...] = mixed.astype(BF16).reshape(NZ, 16, CB)
+    cb[...] = mixed.astype(BF16).reshape(NZ, 16, CBO)
     for d in (4, 3, 5, 2, 6, 1, 7):
         remote(cb.at[along(d)], rcb.at[z], sb4, rb4, at_z(along(d))).start()
     rcb[z] = cb[z]
@@ -514,14 +556,14 @@
     rest = combine - high.astype(F32)
     middle, lowest = in_two(rest)
     all_of(ib2.at[pl.ds(0, NE - 1)], r6)
-    returned = ib2[...].astype(F32).reshape(NE * 8, CA).astype(BF16)
+    returned = ib2[...].astype(F32).reshape(NE * 8, CAO).astype(BF16)
     mix_a = dot(lowest, returned) + dot(middle, returned) + dot(high, returned)
     all_of(rcb.at[pl.ds(0, NZ - 1)], rb4)
-    mix_b = jnp.zeros((16, CB), F32)
+    mix_b = jnp.zeros((16, CBO), F32)
     for zz in range(NZ):
         mix_b = mix_b + rcb[zz].astype(F32)
-    tok_s[:, :CA] = tok_s[:, :CA] + mix_a
-    tok_s[:, CA:] = tok_s[:, CA:] + mix_b
+    tok_s[:, :CAO] = tok_s[:, :CAO] + mix_a
+    tok_s[:, CAO:] = tok_s[:, CAO:] + mix_b
     for c in range(NC):
         result_ref[:, c * CW : (c + 1) * CW] = tok_s[c * TOK : (c + 1) * TOK, :].astype(BF16)
 
@@ -558,21 +600,22 @@
         scratch_shapes=[
             v(tokens.shape, BF16), v((D // W, W), BF16), v((TOK, seqs), I32), v((TOK, TOK), F32),
             v((seqs, W), F32), v((3, seqs, W), BF16), v((NT, W), F32), v((NT, W), BF16), v((D // W, W), BF16), v((TOK, W), BF16),
-            v((D, 2 * W), BF16), v((NC * W, CW), BF16), v((W, W), BF16), v((W, W), BF16),
-            v((DA, 2 * FW), BF16), v((DB, 2 * FW), BF16), v((FW, DA), BF16), v((FW, DB), BF16),
+            v((D, 2 * W), BF16), v((NC * W, CW), BF16), v((2, W, W), BF16),
+            v((DAI, 2 * FW), BF16), v((DBI, 2 * FW), BF16), v((FW, DAO), BF16), v((FW, DBO), BF16),
             v((16, CW), F32), v((NT, 16, CW), BF16),
             v((2, NZ, 16, CW + TAIL), BF16), v((NZ, 16, CW + TAIL), BF16), v((NZ, 16, CW + TAIL), BF16),
             v((NZ, 16, CW + TAIL), BF16),
-            v((NE, 8, CA), BF16), v((NE, 8, CA), BF16),
-            v((NZ, 2, ROWS, DA), BF16), v((NZ, 2 * ROWS, 2 * FW), F32), v((NZ, 2, ROWS, DA), BF16), v((NZ, ROWS, DA), BF16),
-            v((NZ, 2, HALF, DA), BF16), v((2, 4, HALF, DA), BF16), v((2, 4, HALF, DA), BF16),
-            v((NE, 8, CA), BF16), v((NE, 8, CA), BF16), v((16, 4), F32),
-            v((NZ, 16, CB + TAIL), BF16), v((NE, 16, DB), BF16), v((2, NE, 16, DB), BF16), v((NZ, 2, ROWS, DB), BF16),
-            v((2, NZ, ROWS, DB), BF16), v((NZ, ROWS, DB), BF16), v((NE, 16, DB), BF16), v((NE, 16, DB), BF16),
-            v((NZ, 16, CB), BF16), v((NZ, 16, CB), BF16),
-            dma((22,)), dma, dma((NT,)), dma, dma, dma, dma, dma, dma,
-            dma, dma((NZ * 2,)), dma, dma((NZ * 2,)), dma, dma((NZ,)), dma, dma((8,)), dma((8,)), dma, dma,
-            dma, dma, dma, dma((NE,)), dma, dma, dma, dma, dma, dma, dma, dma,
+            v((NE, 8, CAI), BF16), v((NE, 8, CAI), BF16),
+            v((NZ, 2, ROWS, DAI), BF16), v((NZ, 2, ROWS, 2 * FW), F32), v((NZ, 2, ROWS, DAO), BF16), v((NZ, ROWS, DAO), BF16),
+            v((NZ, 4, QUARTER, DAO), BF16), v((4, 4, QUARTER, DAO), BF16), v((4, 4, QUARTER, DAO), BF16),
+            v((NE, 8, CAO), BF16), v((NE, 8, CAO), BF16), v((16, 4), F32),
+            v((256, 256), BF16), v((256, 64), BF16), v((256, 256), BF16), v((256, 256), BF16), v((NC, 128, 256), BF16),
+            v((NZ, 16, CBI + TAIL), BF16), v((NE, 16, DBI), BF16), v((2, NE, 16, DBI), BF16), v((NZ, 2, ROWS, DBI), BF16),
+            v((2, NZ, ROWS, DBO), BF16), v((NZ, ROWS, DBO), BF16), v((NE, 16, DBO), BF16), v((NE, 16, DBO), BF16),
+            v((NZ, 16, CBO), BF16), v((NZ, 16, CBO), BF16),
+            dma((17,)), dma, dma((NZ + 1,)), dma, dma, dma, dma, dma, dma,
+            dma, dma((NZ * 2,)), dma, dma((NZ,)), dma, dma((NZ,)), dma, dma((16,)), dma((16,)), dma, dma,
+            dma, dma, dma, dma((3,)), dma, dma, dma, dma, dma, dma, dma, dma,
         ],
         compiler_params=pltpu.CompilerParams(
             collective_id=0, has_side_effects=True, vmem_limit_bytes=60 * 1024 * 1024
@@ -582,6 +625,25 @@
         decay_logit.reshape(NT, W), rec_gain.reshape(NT, W), second_gain.reshape(D // W, W), conv_taps,
         proj_input, proj_gate, block_decay, block_input, proj_out, expert_gate, expert_up, expert_down,
     )
+    def store(a_ref, b_ref, c_ref, a_hbm, b_hbm, c_hbm, sem):
+        copies = [
+            pltpu.make_async_copy(src, dst, sem.at[i])
+            for i, (src, dst) in enumerate(((a_ref, a_hbm), (b_ref, b_hbm), (c_ref, c_hbm)))
+        ]
+        for copy in copies:
+            copy.start()
+        for copy in copies:
+            copy.wait()
+
+    outs = tuple(pltpu.with_memory_space_constraint(o, pltpu.VMEM) for o in (result, new_state, new_conv))
+    result, new_state, new_conv = pl.pallas_call(
+        store,
+        name="store",
+        out_shape=tuple(jax.ShapeDtypeStruct(o.shape, o.dtype) for o in outs),
+        in_specs=[vmem] * 3,
+        out_specs=(hbm,) * 3,
+        scratch_shapes=[dma((3,))],
+    )(*outs)
     return result, new_state, new_conv.transpose(1, 0, 2)
 
 

time: 85.3 us -> 79.7 us (0.934)
  Pallas kernels: 82.6 us -> 79 us
  local copies, waits for them, and re-layouts: 1.85 us -> 0 us
    pallas_call x1, Pallas kernels: 82.6 us -> 78.3 us  [per_device(): pl.pallas_call(kernel, name='layer', out_shape=(v(tokens.shape, BF16), v(...]
    unnamed x3 -> x0, local copies, waits for them, and re-layouts: 1.85 us -> none
where the time goes in v4:
time: 79.7 us
  Pallas kernels  79 us (99%)
    pallas_call x1, Pallas kernels, per_device(): pl.pallas_call(kernel, name='layer', out_shape=(v(tokens.shape, BF16), v(...  78.3 us

profile of v4, /device:TPU:2, one launch (start us, length us, event | category | flops | bytes accessed | tf_op | source)
XLA Modules:
  0.0 79.7 jit_solution(1768219299184622456)
XLA Ops:
  0.6 78.3 %layer.1 = (bf16[4,4096]{1,0:T(4,128)(2,1)S(1)}, f32[64,128]{1,0:T(8,128)S(1)}, bf16[3,64,128]{2,1,0:T(8,128)(2,1)S(1)}) custom-call(bf16[4,4096]{1,0:T(4,128)(2,1)} %tokens_hbm.1, bf16[32,128]{1,0:T(8,128)(2,1)} %bitcast.8, s32[4,64]{1,0:T(4,128)} %bitcast.12, f32[4,4]{1,0:T(4,128)} %weights_hbm.1, f32[64,128]{1,0:T(8,128)} %rec_hbm.1, ...), custom_call_target="tpu_custom_call" | custom-call | tf_op jit(solution)/shard_map/layer/pallas_call | solution.py:594
  79.0 0.7 store.1

commit v5 on v4

--- a/solution.py
+++ b/solution.py
@@ -80,10 +80,10 @@
     result_ref, state_ref, newconv_ref,
     tokens_ref, gain1_ref, ids_ref, weights_ref, rec_ref, conv_ref, logit_ref, rgain_ref, gain2_ref, taps_ref,
     wcat, w4, gates, wgu_a, wgu_b, wdown_a, wdown_b,
-    tok_s, g1, pb, rp, sb, rb, ob, ib, xa, acc, part_a, rpart_a, sums, rright, rleft, ob2, ib2, rw_s,
+    tok_s, g1, pb, rp, sb, rb, sqs, sqr, ob, ib, xa, acc, part_a, rpart_a, sums, rright, rleft, ob2, ib2, rw_s,
     perm_s, expand_s, by_z_s, by_a_s, chosen_s,
-    sg, tb, xr, xb, part_b, rpart_b, tb2, rr, cb, rcb,
-    lsem, s1, r1, s2p, r2p, s2, r2, s3, r3, s4, r4, s4d, r4d, s5p, r5p, s5, r5r, r5l, s6, r6,
+    sg, tb, xr, acc_b, part_b, rpart_b, tb2, rr, cb, rcb,
+    lsem, s1, s2q, r2q, r1, s2p, r2p, s2, r2, s3, r3, s4, r4, s4d, r4d, s5p, r5p, s5, r5r, r5l, s6, r6,
     sb1, rb1, sb2, rb2, sb2d, rb2d, sbp, rbp, sb3, rb3, sb4, rb4,
 ):
     ep = lax.axis_index("ep")
@@ -278,21 +278,32 @@
     pair2.start()
     pair2.wait_recv()
 
-    def copy2(dev, slot):
-        return pltpu.make_async_remote_copy(
-            src_ref=sb.at[slot], dst_ref=rb.at[z], send_sem=s2, recv_sem=r2, device_id=dev, device_id_type=MESH
-        )
+    row_of, lane_of = iota((NC * TOK, TAIL), 0), iota((NC * TOK, TAIL), 1)
+
+    def in_a_row(zz):
+        total = pb[core, zz, :, CW:].astype(F32) + rp[zz, :, CW:].astype(F32)
+        return jnp.sum(jnp.where(row_of == lane_of, total, 0.0), axis=0, keepdims=True)
 
     for d in (4, 3, 5, 2, 6, 1, 7):
         zz = along(d)
-        sb[zz] = (pb[core, zz].astype(F32) + rp[zz].astype(F32)).astype(BF16)
-        copy2(at_z(zz), zz).start()
-    rb[z] = (pb[core, z].astype(F32) + rp[z].astype(F32)).astype(BF16)
-    pltpu.make_async_copy(sb.at[pl.ds(0, NZ - 1)], rb.at[pl.ds(0, NZ - 1)], r2).wait()
-    summed = jnp.zeros((16, CW + TAIL), F32)
+        sb[zz] = (pb[core, zz, :, :CW].astype(F32) + rp[zz, :, :CW].astype(F32)).astype(BF16)
+        sqs[zz] = in_a_row(zz)
+        remote(sqs.at[zz], sqr.at[z], s2q, r2q, at_z(zz)).start()
+        remote(sb.at[zz], rb.at[z], s2, r2, at_z(zz)).start()
+    sqr[z] = in_a_row(z)
+    rb[z] = (pb[core, z, :, :CW].astype(F32) + rp[z, :, :CW].astype(F32)).astype(BF16)
+    all_of(sqr.at[pl.ds(0, NZ - 1)], r2q)
+    own_row = sqr[0]
+    for zz in range(1, NZ):
+        own_row = own_row + sqr[zz]
+    own_squares = jnp.sum(
+        jnp.where(row_of == lane_of, jnp.broadcast_to(own_row, (NC * TOK, TAIL)), 0.0), axis=1, keepdims=True
+    )
+    all_of(rb.at[pl.ds(0, NZ - 1)], r2)
+    summed = jnp.zeros((16, CW), F32)
     for zz in range(NZ):
         summed = summed + rb[zz].astype(F32)
-    residual = tok_s[...] + summed[:, :CW] * lax.rsqrt(summed[:, CW : CW + 1] * (1.0 / D_REC) + EPS)
+    residual = tok_s[...] + summed * lax.rsqrt(own_squares * (1.0 / D_REC) + EPS)
     scale = lax.rsqrt(per_token(residual * residual) * (1.0 / D) + EPS)
     second = (residual * scale * spread(gain2_ref)).astype(BF16)
     tok_s[...] = residual
@@ -389,8 +400,9 @@
                         copy4(zz, h, nxt).start()
                     cross4(zz, h, core).start()
 
-    def turn_over(side):
-        xb[:, side] = dot(by_z_s[...], xr[side].reshape(rn, DBI)).astype(BF16).reshape(NZ, ROWS, DBI)
+    def other_part(side):
+        rows = dot(by_z_s[...], xr[side].reshape(rn, DBI)).astype(BF16)
+        acc_b[:, side] = dot(rows, wgu_b[...]).reshape(NZ, ROWS, 2 * FW)
 
     arrivals(1)
     first_part(z)
@@ -402,20 +414,19 @@
     first_part(along(2), along(-2))
     across(2 * EARLY, len(ways), 2)
     arrivals(4)
-    turn_over(core)
     all_of(wgu_b, lsem.at[4])
     all_of(wdown_a, lsem.at[5])
     all_of(wdown_b, lsem.at[6])
+    other_part(core)
     first_part(along(3), along(-3), along(4))
     all_of(xr.at[core], rb2d)
-    turn_over(other)
+    other_part(other)
 
     def pair_a(zz):
         return remote(part_a.at[zz, other], rpart_a.at[zz], s5p, r5p.at[zz], mate)
 
     def finish(*blocks):
-        rows = jnp.concatenate([xb[zz].reshape(2 * ROWS, DBI) for zz in blocks], axis=0)
-        gu = jnp.concatenate([acc[zz].reshape(2 * ROWS, 2 * FW) for zz in blocks], axis=0) + dot(rows, wgu_b[...])
+        gu = jnp.concatenate([(acc[zz] + acc_b[zz]).reshape(2 * ROWS, 2 * FW) for zz in blocks], axis=0)
         gate, up = jnp.minimum(gu[:, :FW], CLAMP), jnp.clip(gu[:, FW:], -CLAMP, CLAMP)
         act = ((up + 1.0) * (gate * jax.nn.sigmoid(ALPHA * gate))).astype(BF16)
         out = dot(act, wdown_a[...]).astype(BF16)
@@ -570,6 +581,7 @@
     all_of(g1.at[pl.ds(0, NT - 1)], s1)
     pair2.wait_send()
     all_of(sb.at[pl.ds(0, NZ - 1)], s2)
+    all_of(sqs.at[pl.ds(0, NZ - 1)], s2q)
     all_of(ob.at[pl.ds(0, NE - 1)], s3)
     all_of(xa.at[pl.ds(0, NZ - 1), 0], s4)
     all_of(xa.at[:, 0], s4d)
@@ -603,17 +615,17 @@
             v((D, 2 * W), BF16), v((NC * W, CW), BF16), v((2, W, W), BF16),
             v((DAI, 2 * FW), BF16), v((DBI, 2 * FW), BF16), v((FW, DAO), BF16), v((FW, DBO), BF16),
             v((16, CW), F32), v((NT, 16, CW), BF16),
-            v((2, NZ, 16, CW + TAIL), BF16), v((NZ, 16, CW + TAIL), BF16), v((NZ, 16, CW + TAIL), BF16),
-            v((NZ, 16, CW + TAIL), BF16),
+            v((2, NZ, 16, CW + TAIL), BF16), v((NZ, 16, CW + TAIL), BF16), v((NZ, 16, CW), BF16), v((NZ, 16, CW), BF16),
+            v((NZ, 1, TAIL), F32), v((NZ, 1, TAIL), F32),
             v((NE, 8, CAI), BF16), v((NE, 8, CAI), BF16),
             v((NZ, 2, ROWS, DAI), BF16), v((NZ, 2, ROWS, 2 * FW), F32), v((NZ, 2, ROWS, DAO), BF16), v((NZ, ROWS, DAO), BF16),
             v((NZ, 4, QUARTER, DAO), BF16), v((4, 4, QUARTER, DAO), BF16), v((4, 4, QUARTER, DAO), BF16),
             v((NE, 8, CAO), BF16), v((NE, 8, CAO), BF16), v((16, 4), F32),
             v((256, 256), BF16), v((256, 64), BF16), v((256, 256), BF16), v((256, 256), BF16), v((NC, 128, 256), BF16),
-            v((NZ, 16, CBI + TAIL), BF16), v((NE, 16, DBI), BF16), v((2, NE, 16, DBI), BF16), v((NZ, 2, ROWS, DBI), BF16),
+            v((NZ, 16, CBI + TAIL), BF16), v((NE, 16, DBI), BF16), v((2, NE, 16, DBI), BF16), v((NZ, 2, ROWS, 2 * FW), F32),
             v((2, NZ, ROWS, DBO), BF16), v((NZ, ROWS, DBO), BF16), v((NE, 16, DBO), BF16), v((NE, 16, DBO), BF16),
             v((NZ, 16, CBO), BF16), v((NZ, 16, CBO), BF16),
-            dma((17,)), dma, dma((NZ + 1,)), dma, dma, dma, dma, dma, dma,
+            dma((17,)), dma, dma, dma, dma((NZ + 1,)), dma, dma, dma, dma, dma, dma,
             dma, dma((NZ * 2,)), dma, dma((NZ,)), dma, dma((NZ,)), dma, dma((16,)), dma((16,)), dma, dma,
             dma, dma, dma, dma((3,)), dma, dma, dma, dma, dma, dma, dma, dma,
         ],

time: 79.7 us -> 79.1 us (level)
  no operation moved by 1% of the time
where the time goes in v5:
time: 79.1 us; the launch traced here: 79 us
  Pallas kernels  78.4 us (99%)
    pallas_call x1, Pallas kernels, per_device(): pl.pallas_call(kernel, name='layer', out_shape=(v(tokens.shape, BF16), v(...  77.7 us

profile of v5, /device:TPU:2, one launch (start us, length us, event | category | flops | bytes accessed | tf_op | source)
XLA Modules:
  0.0 79.0 jit_solution(5345810686573120651)
XLA Ops:
  0.6 77.7 %layer.1 = (bf16[4,4096]{1,0:T(4,128)(2,1)S(1)}, f32[64,128]{1,0:T(8,128)S(1)}, bf16[3,64,128]{2,1,0:T(8,128)(2,1)S(1)}) custom-call(bf16[4,4096]{1,0:T(4,128)(2,1)} %tokens_hbm.1, bf16[32,128]{1,0:T(8,128)(2,1)} %bitcast.8, s32[4,64]{1,0:T(4,128)} %bitcast.12, f32[4,4]{1,0:T(4,128)} %weights_hbm.1, f32[64,128]{1,0:T(8,128)} %rec_hbm.1, ...), custom_call_target="tpu_custom_call" | custom-call | tf_op jit(solution)/shard_map/layer/pallas_call | solution.py:606
  78.4 0.7 store.1

commit v6 on v5

--- a/solution.py
+++ b/solution.py
@@ -500,18 +500,15 @@
             pass_on(hop, h, True)
             pass_on(hop, h + 2, False)
 
+    finish(along(4), z)
     finish(along(3), along(-3))
-    finish(along(4), z)
+    pair_a(along(4)).wait_recv()
+    longer(4)
+    finish(along(2), along(-2))
     pair_a(along(3)).wait_recv()
     pair_a(along(-3)).wait_recv()
     shorter(3)
-    finish(along(2), along(-2))
-    pair_a(along(4)).wait_recv()
-    longer(4)
     finish(along(1), along(-1))
-    pair_a(along(2)).wait_recv()
-    pair_a(along(-2)).wait_recv()
-    shorter(2)
 
     half_sum = dot(by_a_s[...], part_b[core].reshape(rn, DBO))
     all_of(rpart_b, rbp)
@@ -521,10 +518,13 @@
     rr[ep] = tb2[ep]
 
     longer(3)
+    pair_a(along(2)).wait_recv()
+    pair_a(along(-2)).wait_recv()
+    shorter(2)
+    longer(2)
     pair_a(along(1)).wait_recv()
     pair_a(along(-1)).wait_recv()
     shorter(1)
-    longer(2)
     longer(1)
     pair_a(z).wait_recv()
     for h in (2, 3, 0, 1):

time: 79.1 us -> 78.2 us (0.989)
  Pallas kernels: 78.4 us -> 76.9 us
    pallas_call x1, Pallas kernels: 77.7 us -> 76.2 us  [per_device(): pl.pallas_call(kernel, name='layer', out_shape=(v(tokens.shape, BF16), v(...]
where the time goes in v6:
time: 78.2 us; the launch traced here: 77.5 us
  Pallas kernels  76.9 us (98%)
    pallas_call x1, Pallas kernels, per_device(): pl.pallas_call(kernel, name='layer', out_shape=(v(tokens.shape, BF16), v(...  76.2 us

profile of v6, /device:TPU:2, one launch (start us, length us, event | category | flops | bytes accessed | tf_op | source)
XLA Modules:
  0.0 77.5 jit_solution(12450592368291974331)
XLA Ops:
  0.6 76.2 %layer.1 = (bf16[4,4096]{1,0:T(4,128)(2,1)S(1)}, f32[64,128]{1,0:T(8,128)S(1)}, bf16[3,64,128]{2,1,0:T(8,128)(2,1)S(1)}) custom-call(bf16[4,4096]{1,0:T(4,128)(2,1)} %tokens_hbm.1, bf16[32,128]{1,0:T(8,128)(2,1)} %bitcast.8, s32[4,64]{1,0:T(4,128)} %bitcast.12, f32[4,4]{1,0:T(4,128)} %weights_hbm.1, f32[64,128]{1,0:T(8,128)} %rec_hbm.1, ...), custom_call_target="tpu_custom_call" | custom-call | tf_op jit(solution)/shard_map/layer/pallas_call | solution.py:606
  76.8 0.7 store.1
